TPU v7x, 256 devices: a whole 4x4x8 slice. The times are simulated.
256 devices in a mesh: ep: 128 (over z, y, x), tp: 2 (over core).
Axes of the slice: x: 4, y: 4, z: 8, core: 2. Of those that a mesh axis runs over, the one named last changes fastest.
Arguments:
- tokens: bfloat16 [32768, 2048], P(('ep', 'tp')), may hold values from -6 to 6
- norm_gain: float32 [2048], replicated, may hold values from 0.25 to 4
- routes: int32 [32768, 2], P(('ep', 'tp')), may hold values from 0 to 127, all different within a row; in each aligned block of 128 rows (0 to 127, 128 to 255, ...) at most 3 rows name the same one
- route_weights: float32 [32768, 2], P(('ep', 'tp')), may hold values from 0.1 to 1
- w_gate: bfloat16 [128, 2048, 1024], P('ep', None, 'tp'), may hold values from -0.125 to 0.125
- w_up: bfloat16 [128, 2048, 1024], P('ep', None, 'tp'), may hold values from -0.125 to 0.125
- w_down: bfloat16 [128, 1024, 2048], P('ep', 'tp'), may hold values from -0.1875 to 0.1875
- dense_in: bfloat16 [2048, 256], P('ep'), may hold values from -0.125 to 0.125
- dense_out: bfloat16 [2048, 256], P('ep'), may hold values from -0.375 to 0.375
- dense_gate: float32 [2048], replicated, may hold values from -6 to 6
Outputs:
- mixed: bfloat16 [32768, 2048], P(('ep', 'tp'))
Inputs may be any that keep to these rules, and one draw needn't show every extreme that they name: `routes`: each row names 2 different experts. Among the 128 rows of one device no expert is named more than 3 times; every draw has a device and an expert with exactly 3.
All inputs are finite; a program needn't handle non-finite values.
Results may differ from a plain program's by a relative error of at most 0.0074.
Values may be sent and summed in bfloat16 or wider, within the bound.
A program may use at most 128 MiB of HBM per device.

v0:
```python
import jax
import jax.numpy as jnp
from jax import lax
from jax.sharding import PartitionSpec as P

CLAMP_LIMIT = 7.0
SLOPE_ALPHA = 1.702
NORM_EPS = 1e-06


def rows_first(arrays, axis, dims):
    turned = [jnp.moveaxis(a, dim, 0) for a, dim in zip(arrays, dims)]
    both = jnp.concatenate([t.reshape(len(t), -1) for t in turned], axis=1)
    out, at, done = (lax.all_gather(both, axis, axis=0, tiled=True), 0, [])
    for t, dim in zip(turned, dims):
        section = out[:, at : at + t[0].size].reshape(-1, *t.shape[1:])
        done.append(jnp.moveaxis(section, 0, dim))
        at += t[0].size
    return tuple(done)


def in_one_piece(arrays, axis, dim, along):
    widths = [a.shape[along] for a in arrays]
    both = jnp.concatenate(arrays, axis=along)
    out = lax.all_gather(both, axis, axis=dim, tiled=True)
    return tuple(jnp.split(out, [sum(widths[:k]) for k in range(1, len(widths))], axis=along))


def rms_normed(tokens, norm_gain):
    widened = tokens.astype(jnp.float32)
    inv_scale = lax.rsqrt(jnp.mean(widened * widened, axis=1, keepdims=True) + NORM_EPS)
    return (widened * inv_scale * norm_gain).astype(jnp.bfloat16)


def clamped_unit(gate_pre, up_pre):
    gate_clip = jnp.minimum(gate_pre, CLAMP_LIMIT)
    up_clip = jnp.clip(up_pre, -CLAMP_LIMIT, CLAMP_LIMIT)
    return ((up_clip + 1.0) * gate_clip * jax.nn.sigmoid(SLOPE_ALPHA * gate_clip)).astype(
        jnp.bfloat16
    )


def rounded_term(hidden_rows, down_rows):
    partial_value = jnp.dot(hidden_rows, down_rows, preferred_element_type=jnp.float32).astype(
        jnp.bfloat16
    )
    return lax.optimization_barrier(partial_value).astype(jnp.float32)


def shards(
    tokens, norm_gain, routes, route_weights, w_gate, w_up, w_down, dense_in, dense_out, dense_gate
):
    tok_rows, model_width = tokens.shape
    top_count = routes.shape[1]
    sources = lax.axis_size("ep")
    experts = sources * w_gate.shape[0]
    core_count = lax.axis_size("tp")
    capacity = (4 * tok_rows * top_count + 3 * experts - 1) // (3 * experts)
    entries = tok_rows * top_count
    normed = rms_normed(tokens, norm_gain)
    flat_routes = routes.reshape(entries)
    onehot = flat_routes[:, None] == lax.broadcasted_iota(jnp.int32, (1, experts), 1)
    earlier_mask = (
        lax.broadcasted_iota(jnp.int32, (entries, entries), 0)
        > lax.broadcasted_iota(jnp.int32, (entries, entries), 1)
    ).astype(jnp.bfloat16)
    counted = jnp.dot(earlier_mask, onehot.astype(jnp.bfloat16), preferred_element_type=jnp.float32)
    slot_index = jnp.sum(jnp.where(onehot, counted, 0.0), axis=1).astype(jnp.int32)
    position = flat_routes * capacity + slot_index
    places = position[None, :] == lax.broadcasted_iota(jnp.int32, (experts * capacity, 1), 0)
    filled = jnp.any(places, axis=1)
    source_entry = jnp.sum(
        jnp.where(places, lax.broadcasted_iota(jnp.int32, (1, entries), 1), 0), axis=1
    )
    buffer = jnp.where(
        filled[:, None], normed[source_entry // top_count], jnp.zeros((), jnp.bfloat16)
    )
    buffer = buffer.reshape(experts, capacity, model_width)
    gate_w = w_gate[0]
    up_w = w_up[0]
    down_w = w_down[0]
    gate_w, up_w, down_w = rows_first((gate_w, up_w, down_w), "tp", (1, 1, 0))
    received = lax.all_to_all(buffer, "ep", split_axis=0, concat_axis=0, tiled=True)
    slot_count = received.shape[1]
    flat_rows = received.reshape(sources * slot_count, model_width)
    hidden = clamped_unit(
        jnp.dot(flat_rows, gate_w, preferred_element_type=jnp.float32),
        jnp.dot(flat_rows, up_w, preferred_element_type=jnp.float32),
    )
    half_width = hidden.shape[1] // core_count
    summed = rounded_term(hidden[:, :half_width], down_w[:half_width])
    summed = summed + rounded_term(
        hidden[:, half_width : half_width + half_width],
        down_w[half_width : half_width + half_width],
    )
    expert_out = summed.astype(jnp.bfloat16).reshape(sources, slot_count, model_width)
    returned = lax.all_to_all(expert_out, "ep", split_axis=0, concat_axis=0, tiled=True)
    flat_returned = returned.reshape(experts * capacity, model_width)
    picked = flat_returned[position].astype(jnp.float32).reshape(tok_rows, top_count, model_width)
    weighted = jnp.sum(picked * route_weights[:, :, None], axis=1)
    whole_in, whole_out = in_one_piece((dense_in, dense_out), "ep", 0, 1)
    dense_hidden = jax.nn.silu(
        jnp.dot(normed, whole_in, preferred_element_type=jnp.float32)
    ).astype(jnp.bfloat16)
    branch = lax.dot_general(
        dense_hidden, whole_out, (((1,), (1,)), ((), ())), preferred_element_type=jnp.float32
    )
    return (weighted + jax.nn.sigmoid(dense_gate) * branch).astype(jnp.bfloat16)


def solution(mesh):
    placed = (
        P(("ep", "tp"), None),
        P(),
        P(("ep", "tp"), None),
        P(("ep", "tp"), None),
        P("ep", None, "tp"),
        P("ep", None, "tp"),
        P("ep", "tp", None),
        P("ep", None),
        P("ep", None),
        P(),
    )
    return jax.shard_map(
        shards, mesh=mesh, in_specs=placed, out_specs=P(("ep", "tp"), None), check_vma=False
    )
```

profile of v0, /device:TPU:32, one launch (start us, length us, event | category | flops | bytes accessed | tf_op | source)
XLA Modules:
  0.0 209.2 jit_solution(5737040500055306987)
XLA Ops:
  6.5 2.9 %copy.21 = bf16[1,2048,512]{1,2,0:T(8,128)(2,1)S(1)} copy(bf16[1,2048,512]{2,1,0:T(8,128)(2,1)} %param.15) | data formatting | bytes 4194304 | tf_op args[5]
  9.5 4.0 %copy.20 = bf16[1,2048,512]{1,2,0:T(8,128)(2,1)} copy(bf16[1,2048,512]{2,1,0:T(8,128)(2,1)} %param.14) | data formatting | bytes 4194304 | tf_op args[4]
  13.4 5.5 %pad_maximum_fusion = bf16[512,6144]{1,0:T(8,128)(2,1)} fusion(bf16[512,2048]{1,0:T(8,128)(2,1)} %bitcast.14, bf16[512,2048]{1,0:T(8,128)(2,1)S(1)} %bitcast.12, bf16[512,2048]{1,0:T(8,128)(2,1)} %bitcast.13), kind=kLoop, calls=%fused_computation.2 | loop fusion | flops 18874368 | bytes 12582912 | tf_op jit(solution)/shard_map/concatenate | solution.py:13
  19.0 0.6 copy-done.6
  19.9 0.2 fusion.10
  20.1 0.1 select_reduce_fusion
  20.3 0.2 fusion.11
  20.5 0.2 fusion.13
  20.7 3.1 %gather_fusion = bf16[384,2048]{1,0:T(8,128)(2,1)} fusion(bf16[128,2048]{1,0:T(8,128)(2,1)S(1)} %fusion.13, s32[1024]{0:T(1024)S(1)} %pad_clamp_fusion.1), kind=kCustom, calls=%fused_computation | custom fusion | bytes 3147264 | tf_op jit(solution)/shard_map/gather | solution.py:76
  23.9 4.0 %gather.9 = bf16[128,3,2048]{2,1,0:T(4,128)(2,1)S(1)} reshape(bf16[384,2048]{1,0:T(8,128)(2,1)} %gather_fusion) | data formatting | bytes 3145728 | tf_op jit(solution)/shard_map/gather | solution.py:76
  27.9 0.2 fusion.19
  28.0 0.2 broadcast_in_dim.39
  28.3 2.3 %broadcast_select_fusion = bf16[128,3,2048]{2,1,0:T(4,128)(2,1)} fusion(bf16[128,3,2048]{2,1,0:T(4,128)(2,1)S(1)} %gather.9, pred[128,3]{1,0:T(8,128)(4,1)S(1)} %broadcast_in_dim.39), kind=kLoop, calls=%fused_computation.16 | loop fusion | flops 786432 | bytes 3146112 | tf_op jit(solution)/shard_map/jit(_where)/select_n | solution.py:75
  30.6 15.1 %all-to-all-start = ((bf16[128,3,2048]{2,1,0:T(4,128)(2,1)}), bf16[128,3,2048]{2,1,0:T(4,128)(2,1)S(1)}, u32[]{:S(2)}, u32[]{:S(2)}) async-start(bf16[128,3,2048]{2,1,0:T(4,128)(2,1)} %broadcast_select_fusion), calls=%async_computation | async-start | bytes 4194304 | tf_op jit(solution)/shard_map/all_to_all | solution.py:83
  45.7 0.2 all-gather.5.cloned.1.call-start
  46.0 0.6 pad_maximum_fusion.1
  46.6 52.8 %all-to-all-done = bf16[128,3,2048]{2,1,0:T(4,128)(2,1)S(1)} async-done(((bf16[128,3,2048]{2,1,0:T(4,128)(2,1)}), bf16[128,3,2048]{2,1,0:T(4,128)(2,1)S(1)}, u32[]{:S(2)}, u32[]{:S(2)}) %all-to-all-start) | async-done | bytes 1572896 | tf_op jit(solution)/shard_map/all_to_all | solution.py:83
  99.4 2.5 %reshape.136 = bf16[384,2048]{1,0:T(8,128)(2,1)} reshape(bf16[128,3,2048]{2,1,0:T(4,128)(2,1)S(1)} %all-to-all-done) | data formatting | bytes 3145728 | tf_op jit(solution)/shard_map/reshape | solution.py:85
  101.9 4.6 %fusion = f32[384,1024]{1,0:T(8,128)S(1)} fusion(bf16[384,2048]{1,0:T(8,128)(2,1)} %reshape.136, bf16[1024,6144]{1,0:T(8,128)(2,1)} %all-gather.3.cloned.1.call-done), kind=kOutput, calls=%fused_computation.3 | convolution fusion | flops 1610612736 | bytes 7340032 | tf_op jit(solution)/shard_map/dot_general | solution.py:87
  106.5 4.3 %multiply_convert_fusion = bf16[384,1024]{1,0:T(8,128)(2,1)S(1)} fusion(f32[384,1024]{1,0:T(8,128)S(1)} %fusion, bf16[384,2048]{1,0:T(8,128)(2,1)S(1)} %copy-done.1, bf16[1024,6144]{1,0:T(8,128)(2,1)} %all-gather.3.cloned.1.call-done), kind=kOutput, calls=%fused_computation.17 | convolution fusion | flops 1614544896 | bytes 8126464 | tf_op jit(solution)/shard_map/dot_general | solution.py:88
  110.9 2.6 %convolution_convert_fusion = bf16[384,2048]{1,0:T(8,128)(2,1)S(1)} fusion(bf16[1024,6144]{1,0:T(8,128)(2,1)} %all-gather.3.cloned.1.call-done, bf16[384,1024]{1,0:T(8,128)(2,1)S(1)} %multiply_convert_fusion), kind=kOutput, calls=%fused_computation.8 | convolution fusion | flops 806092800 | bytes 4063232 | tf_op jit(solution)/shard_map/dot_general | solution.py:44
  113.5 2.6 %convolution_convert_fusion.1 = bf16[384,2048]{1,0:T(8,128)(2,1)S(1)} fusion(bf16[1024,6144]{1,0:T(8,128)(2,1)} %all-gather.3.cloned.1.call-done, bf16[384,1024]{1,0:T(8,128)(2,1)S(1)} %multiply_convert_fusion), kind=kOutput, calls=%fused_computation.9 | convolution fusion | flops 806092800 | bytes 4063232 | tf_op jit(solution)/shard_map/dot_general | solution.py:44
  116.1 0.6 add_convert_fusion
  116.7 2.3 %reshape.137 = bf16[128,3,2048]{2,1,0:T(4,128)(2,1)} reshape(bf16[384,2048]{1,0:T(8,128)(2,1)S(1)} %add_convert_fusion) | data formatting | bytes 3145728 | tf_op jit(solution)/shard_map/reshape | solution.py:96
  119.0 7.2 %all-to-all-start.1 = ((bf16[128,3,2048]{2,1,0:T(4,128)(2,1)}), bf16[128,3,2048]{2,1,0:T(4,128)(2,1)}, u32[]{:S(2)}, u32[]{:S(2)}) async-start(bf16[128,3,2048]{2,1,0:T(4,128)(2,1)} %reshape.137), calls=%async_computation.1 | async-start | bytes 4194304 | tf_op jit(solution)/shard_map/all_to_all | solution.py:97
  126.3 0.1 mul.88
  126.7 59.4 %all-to-all-done.1 = bf16[128,3,2048]{2,1,0:T(4,128)(2,1)} async-done(((bf16[128,3,2048]{2,1,0:T(4,128)(2,1)}), bf16[128,3,2048]{2,1,0:T(4,128)(2,1)}, u32[]{:S(2)}, u32[]{:S(2)}) %all-to-all-start.1) | async-done | bytes 1572896 | tf_op jit(solution)/shard_map/all_to_all | solution.py:97
  186.0 3.9 %reshape.138 = bf16[384,2048]{1,0:T(8,128)(2,1)S(1)} reshape(bf16[128,3,2048]{2,1,0:T(4,128)(2,1)} %all-to-all-done.1) | data formatting | bytes 3145728 | tf_op jit(solution)/shard_map/reshape | solution.py:98
  190.0 2.3 %gather_fusion.1 = bf16[256,2048]{1,0:T(8,128)(2,1)} fusion(bf16[384,2048]{1,0:T(8,128)(2,1)S(1)} %reshape.138, s32[1024]{0:T(1024)S(1)} %pad_clamp_fusion), kind=kCustom, calls=%fused_computation.1 | custom fusion | bytes 2098176 | tf_op jit(solution)/shard_map/gather | solution.py:99
  192.3 2.4 %reshape.139 = f32[128,2,2048]{2,1,0:T(2,128)S(1)} reshape(bf16[256,2048]{1,0:T(8,128)(2,1)} %gather_fusion.1) | data formatting | bytes 3145728 | tf_op jit(solution)/shard_map/convert_element_type | solution.py:99
  194.7 4.1 %multiply_reduce_fusion = f32[128,2048]{1,0:T(8,128)} fusion(f32[128,2,2048]{2,1,0:T(2,128)S(1)} %reshape.139, f32[128,2]{1,0:T(8,128)S(1)} %copy.23), kind=kLoop, calls=%fused_computation.15 | loop fusion | flops 786432 | bytes 3146752 | tf_op jit(solution)/shard_map/reduce_sum | solution.py:100
  198.8 3.6 %fusion.5 = bf16[128,2048]{1,0:T(8,128)(2,1)} fusion(f32[128,2048]{1,0:T(8,128)} %multiply_reduce_fusion, bf16[2048,512]{1,0:T(8,128)(2,1)} %all-gather.5.cloned.1.call-done, f32[2048]{0:T(1024)S(1)} %add_divide_fusion, bf16[128,2048]{1,0:T(8,128)(2,1)S(1)} %fusion.13), kind=kOutput, calls=%fused_computation.12 | convolution fusion | flops 269385728 | bytes 4202496 | tf_op jit(solution)/shard_map/dot_general | solution.py:105
  (33 shorter events, 0.6 us)
Async XLA Ops:
  6.5 95.4 %all-gather.3.cloned.1.call-start = ((), (), s32[]{:S(2)}) async-start(), calls=%async_computation.2 | async-start | bytes 18874368 | tf_op jit(solution)/shard_map/all_gather | solution.py:14
  19.0 0.7 copy-start.6
  19.0 1.4 copy-start
  19.0 1.6 copy-start.2
  30.6 15.4 %copy-start.4 = (bf16[16,256]{1,0:T(8,128)(2,1)S(1)}, bf16[16,256]{1,0:T(8,128)(2,1)}, u32[]{:S(2)}) copy-start(bf16[16,256]{1,0:T(8,128)(2,1)} %param.18) | copy-start | bytes 24580
  30.6 15.4 %copy-start.5 = (bf16[16,256]{1,0:T(8,128)(2,1)S(1)}, bf16[16,256]{1,0:T(8,128)(2,1)}, u32[]{:S(2)}) copy-start(bf16[16,256]{1,0:T(8,128)(2,1)} %param.17) | copy-start | bytes 24580
  30.6 68.8 %all-to-all-start = ((bf16[128,3,2048]{2,1,0:T(4,128)(2,1)}), bf16[128,3,2048]{2,1,0:T(4,128)(2,1)S(1)}, u32[]{:S(2)}, u32[]{:S(2)}) async-start(bf16[128,3,2048]{2,1,0:T(4,128)(2,1)} %broadcast_select_fusion), calls=%async_computation | async-start | bytes 4194304 | tf_op jit(solution)/shard_map/all_to_all | solution.py:83
  45.7 153.0 %all-gather.5.cloned.1.call-start = ((), (), s32[]{:S(2)}) async-start(), calls=%async_computation.3 | async-start | bytes 2113536 | tf_op jit(solution)/shard_map/all_gather | solution.py:25
  101.9 4.6 %copy-start.1 = (bf16[384,2048]{1,0:T(8,128)(2,1)S(1)}, bf16[384,2048]{1,0:T(8,128)(2,1)}, u32[]{:S(2)}) copy-start(bf16[384,2048]{1,0:T(8,128)(2,1)} %reshape.136) | copy-start | bytes 4718596
  119.0 7.5 %copy-start.7 = (f32[128,2]{0,1:T(2,128)S(1)}, f32[128,2]{0,1:T(2,128)}, u32[]{:S(2)}) copy-start(f32[128,2]{0,1:T(2,128)} %param.13) | copy-start | bytes 3076
  119.0 7.6 %copy-start.3 = (f32[2048]{0:T(1024)S(1)}, f32[2048]{0:T(1024)}, u32[]{:S(2)}) copy-start(f32[2048]{0:T(1024)} %param.19) | copy-start | bytes 24580
  119.0 67.0 %all-to-all-start.1 = ((bf16[128,3,2048]{2,1,0:T(4,128)(2,1)}), bf16[128,3,2048]{2,1,0:T(4,128)(2,1)}, u32[]{:S(2)}, u32[]{:S(2)}) async-start(bf16[128,3,2048]{2,1,0:T(4,128)(2,1)} %reshape.137), calls=%async_computation.1 | async-start | bytes 4194304 | tf_op jit(solution)/shard_map/all_to_all | solution.py:97
Sparse Core Ops, SparseCore 0:
  19.1 32.6 all-gather.2
  55.4 122.7 all-gather.4
where the time goes:
time: 210 us; the launch traced here: 209 us
  waiting for transfers between devices  112 us (53%)
  local copies, waits for them, and re-layouts  29 us (14%)
  starting transfers between devices  22.6 us (11%)
  matrix products  17.9 us (9%)
  other arithmetic  13.9 us (7%)
  between operations  13.6 us (6%)
    all_to_all x1, waiting for transfers between devices, shards(): lax.all_to_all(expert_out, 'ep', split_axis=0, concat_axis=0, tiled=True)  59.4 us
    all_to_all x1, waiting for transfers between devices, shards(): lax.all_to_all(buffer, 'ep', split_axis=0, concat_axis=0, tiled=True)  52.8 us
    all_to_all x1, starting transfers between devices, shards(): lax.all_to_all(buffer, 'ep', split_axis=0, concat_axis=0, tiled=True)  15.1 us
    unnamed x20, local copies, waits for them, and re-layouts  7.79 us
    all_to_all x1, starting transfers between devices, shards(): lax.all_to_all(expert_out, 'ep', split_axis=0, concat_axis=0, tiled=True)  7.19 us
    gather x2, local copies, waits for them, and re-layouts, shards(): normed[source_entry // top_count]  7.1 us
    concatenate x1, other arithmetic, rows_first(): both = jnp.concatenate([t.reshape(len(t), -1) for t in turned], axis=1)  5.51 us
    dot_general x2, matrix products, rounded_term(): jnp.dot(hidden_rows, down_rows, preferred_element_type=jnp.float32)  5.18 us
  transfers between devices with their start and end apart: 4, of which 2 were waited for; matrix products, arithmetic and copies ran while one was open for 21% of the time, Pallas kernels for 0%

commit v1 on v0

v1 whole, which is shorter than its diff:
```python
import jax
import jax.numpy as jnp
from jax import lax
from jax.experimental import pallas as pl
from jax.experimental.pallas import tpu as pltpu
from jax.sharding import PartitionSpec as P

CLAMP_LIMIT = 7.0
SLOPE_ALPHA = 1.702
NORM_EPS = 1e-06
MESH = pl.DeviceIdType.MESH
BF16 = jnp.bfloat16
F32 = jnp.float32

PEERS = 128
CAP = 3
LANES = 128
SUB = 16
SELF = 7
GROUPS = 2
PER_GROUP = PEERS // GROUPS
ROWS = PER_GROUP * CAP
PACK = 16


def place_of(dz, dy, dx):
    j = jnp.where(dz == 0, 0, jnp.where(dz <= 4, 2 * dz - 1, 2 * (8 - dz)))
    return (dy * 4 + dx) * 8 + 7 - j


def offset_of(k):
    j = 7 - lax.rem(k, 8)
    odd = lax.rem(j, 2)
    half = lax.div(j, 2)
    dz = lax.rem(odd * (half + 1) + (1 - odd) * (8 - half), 8)
    r = lax.div(k, 8)
    return dz, lax.div(r, 4), lax.rem(r, 4)


def clamped_unit(gate_pre, up_pre):
    gate_clip = jnp.minimum(gate_pre, CLAMP_LIMIT)
    up_clip = jnp.clip(up_pre, -CLAMP_LIMIT, CLAMP_LIMIT)
    return ((up_clip + 1.0) * gate_clip * jax.nn.sigmoid(SLOPE_ALPHA * gate_clip)).astype(BF16)


def kernel(
    src_ref, pos_ref, rw_ref, tok_hbm, gain_ref, dgate_ref, wg_hbm, wu_hbm, wd_hbm, din_hbm, dout_hbm,
    o_ref,
    tok, x2, x3, send, recv, xg, hid, acc, outb, ret, wg, wu, wd, wgo, wuo, wdo, dense, branch,
    tok_sem, w_sem, wsend_sem, wrecv_sem, d_sem, dsend_sem, drecv_sem,
    send_sem, recv_sem, rsend_sem, rrecv_sem,
):
    me = lax.axis_index("ep")
    tp = lax.axis_index("tp")
    z, y, x = lax.div(me, 16), lax.rem(lax.div(me, 4), 4), lax.rem(me, 4)

    def chip(dz, dy, dx):
        return (
            lax.rem(z + dz, 8) * 16 + lax.rem(y + dy, 4) * 4 + lax.rem(x + dx, 4)
        )

    def back(dz, dy, dx):
        return (
            lax.rem(z + 8 - dz, 8) * 16 + lax.rem(y + 4 - dy, 4) * 4 + lax.rem(x + 4 - dx, 4)
        )

    tok_copy = pltpu.make_async_copy(tok_hbm, tok, tok_sem)
    tok_copy.start()

    @pl.when(tp == 0)
    def _():
        pltpu.make_async_copy(din_hbm, dense.at[0, z, y, x], d_sem).start()

    @pl.when(tp == 1)
    def _():
        pltpu.make_async_copy(dout_hbm, dense.at[1, z, y, x], d_sem).start()

    barrier = pltpu.get_barrier_semaphore()

    def greet(k, c):
        pl.semaphore_signal(
            barrier, inc=1, device_id=(lax.rem(me + k, PEERS), tp), device_id_type=MESH
        )
        return c

    lax.fori_loop(1, PEERS, greet, 0)
    pl.semaphore_signal(barrier, inc=1, device_id=(me, 1 - tp), device_id_type=MESH)

    own = [
        pltpu.make_async_copy(a, b, w_sem.at[i])
        for i, (a, b) in enumerate(((wg_hbm, wg), (wu_hbm, wu), (wd_hbm, wd)))
    ]
    other = [
        pltpu.make_async_remote_copy(
            src_ref=a, dst_ref=b, send_sem=wsend_sem.at[i], recv_sem=wrecv_sem.at[i],
            device_id=(me, 1 - tp), device_id_type=MESH,
        )
        for i, (a, b) in enumerate(((wg_hbm, wgo), (wu_hbm, wuo), (wd_hbm, wdo)))
    ]

    tok_copy.wait()
    for copy in own:
        copy.start()

    for i in range(8):
        rows = slice(i * 16, i * 16 + 16)
        wide = tok[rows, :].astype(F32)
        scale = lax.rsqrt(jnp.mean(wide * wide, axis=1, keepdims=True) + NORM_EPS)
        normed = (wide * scale * gain_ref[...]).astype(BF16)
        x2[rows, :] = normed
        x3[rows] = normed.reshape(16, SUB, LANES)

    pltpu.make_async_copy(din_hbm, dense.at[tp, z, y, x], d_sem).wait()
    pl.semaphore_wait(barrier, PEERS)

    def spread(stage, count, block, target):
        def one(d, c):
            pltpu.make_async_remote_copy(
                src_ref=block, dst_ref=block, send_sem=dsend_sem.at[stage],
                recv_sem=drecv_sem.at[stage], device_id=(target(d), tp), device_id_type=MESH,
            ).start()
            return c

        lax.fori_loop(1, count, one, 0)

    z_block = dense.at[tp, z, y, x]
    y_block = dense.at[tp, :, y, x]
    x_block = dense.at[tp, :, :, x]
    z_all = dense.at[tp, pl.ds(0, 7), y, x]
    y_all = dense.at[tp, :, pl.ds(0, 3), x]
    x_all = dense.at[tp, :, :, pl.ds(0, 3)]

    def all_in(ref, sem):
        pltpu.make_async_copy(ref, ref, sem).wait()

    spread(0, 8, z_block, lambda d: chip(d, 0, 0))

    def pack(k, c):
        for s in range(CAP):
            send[k * CAP + s] = x3[src_ref[k * CAP + s]]
        return c

    def dispatch(k, c):
        rows = pl.ds(k * CAP, CAP)

        @pl.when(k != SELF)
        def _():
            pltpu.make_async_remote_copy(
                src_ref=send.at[rows], dst_ref=recv.at[rows], send_sem=send_sem,
                recv_sem=recv_sem.at[lax.div(k, PER_GROUP)],
                device_id=(chip(*offset_of(k)), tp), device_id_type=MESH,
            ).start()

        return c

    def pack_and_send(first, last):
        lax.fori_loop(first, first + PACK, pack, 0)

        def step(b, c):
            lax.fori_loop(b * PACK + PACK, b * PACK + 2 * PACK, pack, 0)
            lax.fori_loop(b * PACK, b * PACK + PACK, dispatch, 0)
            return c

        lax.fori_loop(first // PACK, last // PACK - 1, step, 0)
        lax.fori_loop(last - PACK, last, dispatch, 0)

    pack_and_send(0, PER_GROUP)
    for s in range(CAP):
        recv[SELF * CAP + s] = send[SELF * CAP + s]

    all_in(z_all, drecv_sem.at[0])
    spread(1, 4, y_block, lambda d: chip(0, d, 0))
    pack_and_send(PER_GROUP, PEERS)
    for copy in other:
        copy.start()
    all_in(y_all, drecv_sem.at[1])
    spread(2, 4, x_block, lambda d: chip(0, 0, d))

    def answer(k, c):
        rows = pl.ds(k * CAP, CAP)

        @pl.when(k != SELF)
        def _():
            pltpu.make_async_remote_copy(
                src_ref=outb.at[rows], dst_ref=ret.at[rows], send_sem=rsend_sem,
                recv_sem=rrecv_sem.at[lax.div(k, PER_GROUP)],
                device_id=(back(*offset_of(k)), tp), device_id_type=MESH,
            ).start()

        return c

    def group_bytes(g):
        return PER_GROUP - 1 if g == 0 else PER_GROUP

    for g in range(GROUPS):
        base = g * ROWS
        all_in(recv.at[pl.ds(0, group_bytes(g) * CAP)], recv_sem.at[g])

        for r in range(0, ROWS, 16):
            xg[r : r + 16, :] = recv[base + r : base + r + 16].reshape(16, SUB * LANES)

        for h, (gate_w, up_w) in enumerate(((wg, wu), (wgo, wuo))):
            if g == 0:
                if h == 0:
                    for copy in own:
                        copy.wait()
                else:
                    for copy in other:
                        copy.wait_recv()
            for t in range(2):
                cols = slice(t * 256, t * 256 + 256)
                hid[:, h * 512 + t * 256 : h * 512 + t * 256 + 256] = clamped_unit(
                    jnp.dot(xg[...], gate_w[:, cols], preferred_element_type=F32),
                    jnp.dot(xg[...], up_w[:, cols], preferred_element_type=F32),
                )

        for t in range(8):
            cols = slice(t * 256, t * 256 + 256)
            first = jnp.dot(hid[:, :512], wd[:, cols], preferred_element_type=F32).astype(BF16)
            second = jnp.dot(hid[:, 512:], wdo[:, cols], preferred_element_type=F32).astype(BF16)
            summed = first.astype(F32) + second.astype(F32)
            for i in range(2):
                acc[pl.ds(2 * t + i, ROWS, stride=SUB), :] = summed[:, i * LANES : (i + 1) * LANES]

        for r in range(0, ROWS, 16):
            outb[base + r : base + r + 16] = (
                acc[r * SUB : (r + 16) * SUB, :].reshape(16, SUB, LANES).astype(BF16)
            )

        lax.fori_loop(g * PER_GROUP, (g + 1) * PER_GROUP, answer, 0)

    for s in range(CAP):
        ret[SELF * CAP + s] = outb[SELF * CAP + s]

    all_in(x_all, drecv_sem.at[2])
    swap = pltpu.make_async_remote_copy(
        src_ref=dense.at[tp], dst_ref=dense.at[tp], send_sem=dsend_sem.at[3],
        recv_sem=drecv_sem.at[3], device_id=(me, 1 - tp), device_id_type=MESH,
    )
    swap.start()
    swap.wait_recv()

    pre = jnp.zeros((128, 256), F32)
    for i in range(8):
        pre = pre + jnp.dot(
            x2[:, i * 256 : (i + 1) * 256], dense[0, i].reshape(256, 256), preferred_element_type=F32
        )
    dense_hidden = jax.nn.silu(pre).astype(BF16)
    for i in range(8):
        part = lax.dot_general(
            dense_hidden, dense[1, i].reshape(256, 256), (((1,), (1,)), ((), ())),
            preferred_element_type=F32,
        )
        for j in range(2):
            branch[pl.ds(2 * i + j, 128, stride=SUB), :] = part[:, j * LANES : (j + 1) * LANES]

    gate = jax.nn.sigmoid(dgate_ref[...])
    for g in range(GROUPS):
        all_in(ret.at[pl.ds(0, group_bytes(g) * CAP)], rrecv_sem.at[g])

    @pl.loop(0, 128)
    def _(t):
        weighted = (
            rw_ref[2 * t] * ret[pos_ref[2 * t]].astype(F32)
            + rw_ref[2 * t + 1] * ret[pos_ref[2 * t + 1]].astype(F32)
        )
        tile = pl.ds(pl.multiple_of(t * SUB, SUB), SUB)
        o_ref[t] = (weighted + gate * branch[tile, :]).astype(BF16)

    all_in(send.at[pl.ds(0, (PEERS - 1) * CAP)], send_sem)
    all_in(outb.at[pl.ds(0, (PEERS - 1) * CAP)], rsend_sem)
    for copy in other:
        copy.wait_send()
    all_in(z_all, dsend_sem.at[0])
    all_in(y_all, dsend_sem.at[1])
    all_in(x_all, dsend_sem.at[2])
    swap.wait_send()


def tables(routes):
    rows, top = routes.shape
    entries = rows * top
    me = lax.axis_index("ep")
    flat = routes.reshape(entries)
    onehot = flat[:, None] == lax.broadcasted_iota(jnp.int32, (1, PEERS), 1)
    earlier = (
        lax.broadcasted_iota(jnp.int32, (entries, entries), 0)
        > lax.broadcasted_iota(jnp.int32, (entries, entries), 1)
    ).astype(BF16)
    counted = jnp.dot(earlier, onehot.astype(BF16), preferred_element_type=F32)
    slot = jnp.sum(jnp.where(onehot, counted, 0.0), axis=1).astype(jnp.int32)
    dz = (flat // 16 - me // 16) % 8
    dy = (flat // 4 % 4 - me // 4 % 4) % 4
    dx = (flat % 4 - me % 4) % 4
    position = place_of(dz, dy, dx) * CAP + slot
    places = position[None, :] == lax.broadcasted_iota(jnp.int32, (PEERS * CAP, 1), 0)
    source = jnp.sum(
        jnp.where(places, lax.broadcasted_iota(jnp.int32, (1, entries), 1) // top, 0), axis=1
    )
    return source, position


def shards(
    tokens, norm_gain, routes, route_weights, w_gate, w_up, w_down, dense_in, dense_out, dense_gate
):
    source, position = tables(routes)
    smem = pl.BlockSpec(memory_space=pltpu.SMEM)
    vmem = pl.BlockSpec(memory_space=pltpu.VMEM)
    hbm = pl.BlockSpec(memory_space=pl.ANY)
    dma = pltpu.SemaphoreType.DMA
    out = pl.pallas_call(
        kernel,
        out_shape=jax.ShapeDtypeStruct((128, SUB, LANES), BF16),
        in_specs=[smem, smem, smem, hbm, vmem, vmem, hbm, hbm, hbm, hbm, hbm],
        out_specs=vmem,
        scratch_shapes=[
            pltpu.VMEM((128, 2048), BF16),
            pltpu.VMEM((128, 2048), BF16),
            pltpu.VMEM((128, SUB, LANES), BF16),
            pltpu.VMEM((PEERS * CAP, SUB, LANES), BF16),
            pltpu.VMEM((PEERS * CAP, SUB, LANES), BF16),
            pltpu.VMEM((ROWS, 2048), BF16),
            pltpu.VMEM((ROWS, 1024), BF16),
            pltpu.VMEM((ROWS * SUB, LANES), F32),
            pltpu.VMEM((PEERS * CAP, SUB, LANES), BF16),
            pltpu.VMEM((PEERS * CAP, SUB, LANES), BF16),
            pltpu.VMEM((2048, 512), BF16),
            pltpu.VMEM((2048, 512), BF16),
            pltpu.VMEM((512, 2048), BF16),
            pltpu.VMEM((2048, 512), BF16),
            pltpu.VMEM((2048, 512), BF16),
            pltpu.VMEM((512, 2048), BF16),
            pltpu.VMEM((2, 8, 4, 4, 16, 256), BF16),
            pltpu.VMEM((128 * SUB, LANES), F32),
            dma, dma((3,)), dma((3,)), dma((3,)), dma, dma((4,)), dma((4,)),
            dma, dma((GROUPS,)), dma, dma((GROUPS,)),
        ],
        compiler_params=pltpu.CompilerParams(
            collective_id=0, has_side_effects=True, vmem_limit_bytes=56 << 20
        ),
    )(
        source, position, route_weights.reshape(-1), tokens, norm_gain.reshape(1, -1),
        dense_gate.reshape(SUB, LANES), w_gate[0], w_up[0], w_down[0], dense_in, dense_out,
    )
    return out.reshape(tokens.shape)


def solution(mesh):
    placed = (
        P(("ep", "tp"), None),
        P(),
        P(("ep", "tp"), None),
        P(("ep", "tp"), None),
        P("ep", None, "tp"),
        P("ep", None, "tp"),
        P("ep", "tp", None),
        P("ep", None),
        P("ep", None),
        P(),
    )
    return jax.shard_map(
        shards, mesh=mesh, in_specs=placed, out_specs=P(("ep", "tp"), None), check_vma=False
    )
```

time: 210 us -> 93.3 us (0.44)
  waiting for transfers between devices: 112 us -> 0 us
  Pallas kernels: 0 us -> 87.4 us
  local copies, waits for them, and re-layouts: 29 us -> 4.37 us
  starting transfers between devices: 22.6 us -> 0 us
  matrix products: 17.9 us -> 0.24 us
  between operations: 13.6 us -> 0.03 us
  other arithmetic: 13.9 us -> 0.76 us
    all_to_all x2 -> x0, waiting for transfers between devices: 112 us -> none  [the longest x1 59.4 us: shards(): lax.all_to_all(expert_out, 'ep', split_axis=0, concat_axis=0, tiled=True)]
    pallas_call x0 -> x1, Pallas kernels: none -> 87.4 us  [shards(): pl.pallas_call(kernel, out_shape=jax.ShapeDtypeStruct((128, SUB, LANES),...]
    all_to_all x2 -> x0, starting transfers between devices: 22.3 us -> none  [the longest x1 15.1 us: shards(): lax.all_to_all(buffer, 'ep', split_axis=0, concat_axis=0, tiled=True)]
    dot_general x6 -> x1, matrix products: 17.9 us -> 0.24 us  [tables(): counted = jnp.dot(earlier, onehot.astype(BF16), preferred_element_type=F32)]
    gather x3 -> x0, local copies, waits for them, and re-layouts: 9.45 us -> none  [the longest x2 7.1 us: shards(): normed[source_entry // top_count]]
    reshape x4 -> x2, local copies, waits for them, and re-layouts: 8.91 us -> 0.82 us  [the longest x1 0.69 us: shards(): route_weights.reshape(-1)]
    concatenate x2 -> x0, other arithmetic: 6.12 us -> none  [the longest x1 5.51 us: rows_first(): both = jnp.concatenate([t.reshape(len(t), -1) for t in turned], axis=1)]
    unnamed x20 -> x5, local copies, waits for them, and re-layouts: 7.79 us -> 3.54 us
  transfers between devices with their start and end apart: 4 -> 0, of which waited for: 2 -> 0; matrix products, arithmetic and copies ran while one was open for 21% -> 0% of each run, Pallas kernels for 0% -> 0%
where the time goes in v1:
time: 93.3 us; the launch traced here: 92.8 us
  Pallas kernels  87.4 us (94%)
  local copies, waits for them, and re-layouts  4.37 us (5%)
    pallas_call x1, Pallas kernels, shards(): pl.pallas_call(kernel, out_shape=jax.ShapeDtypeStruct((128, SUB, LANES),...  87.4 us
    unnamed x5, local copies, waits for them, and re-layouts  3.54 us

profile of v1, /device:TPU:32, one launch (start us, length us, event | category | flops | bytes accessed | tf_op | source)
XLA Modules:
  0.0 92.8 jit_solution(3474753584637634591)
XLA Ops:
  0.0 0.8 copy.13
  0.8 0.1 reshape.176
  0.9 0.2 fusion
  1.2 0.0 copy-start
  1.2 0.7 select_reduce_fusion.src_ref
  1.9 0.8 copy.14
  2.7 0.7 reshape.177.rw_ref
  3.4 0.0 copy-done
  3.4 87.4 %shard_map.100 = bf16[128,16,128]{2,1,0:T(8,128)(2,1)} custom-call(s32[384]{0:T(512)} %select_reduce_fusion.src_ref, s32[256]{0:T(256)} %copy-done, f32[256]{0:T(256)} %reshape.177.rw_ref, bf16[128,2048]{1,0:T(8,128)(2,1)} %tok_hbm.1, f32[1,2048]{1,0:T(1,128)} %bitcast.13, f32[16,128]{1,0:T(8,128)} %bitcast.14, bf16[2048,512]{1,0:T(8,128)(2,1)} %bitcast.9, ...), custom_call_target="tpu_custom_call" | custom-call | tf_op jit(solution)/shard_map/pallas_call | solution.py:311
  90.8 2.0 %copy.17 = bf16[16,8,16,128]{3,1,2,0:T(8,128)(2,1)} copy(bf16[16,8,16,128]{3,2,1,0:T(8,128)(2,1)} %bitcast.12) | data formatting | bytes 1048576
  (1 shorter events, 0.0 us)
Async XLA Ops:
  1.2 2.2 %copy-start = (s32[256]{0:T(256)}, s32[256]{0:T(256)S(1)}, u32[]{:S(2)}) copy-start(s32[256]{0:T(256)S(1)} %get-tuple-element.6.pos_ref) | copy-start | bytes 3076

commit v2 on v1

--- a/solution.py
+++ b/solution.py
@@ -25,7 +25,7 @@
 
 def place_of(dz, dy, dx):
     j = jnp.where(dz == 0, 0, jnp.where(dz <= 4, 2 * dz - 1, 2 * (8 - dz)))
-    return (dy * 4 + dx) * 8 + 7 - j
+    return (dx * 4 + dy) * 8 + 7 - j
 
 
 def offset_of(k):
@@ -34,7 +34,7 @@
     half = lax.div(j, 2)
     dz = lax.rem(odd * (half + 1) + (1 - odd) * (8 - half), 8)
     r = lax.div(k, 8)
-    return dz, lax.div(r, 4), lax.rem(r, 4)
+    return dz, lax.rem(r, 4), lax.div(r, 4)
 
 
 def clamped_unit(gate_pre, up_pre):
@@ -44,9 +44,11 @@
 
 
 def kernel(
-    src_ref, pos_ref, rw_ref, tok_hbm, gain_ref, dgate_ref, wg_hbm, wu_hbm, wd_hbm, din_hbm, dout_hbm,
-    o_ref,
-    tok, x2, x3, send, recv, xg, hid, acc, outb, ret, wg, wu, wd, wgo, wuo, wdo, dense, branch,
+    routes_hbm, rw_hbm, tok_hbm, gain_hbm, dgate_hbm, wg_hbm, wu_hbm, wd_hbm, din_hbm, dout_hbm,
+    o_hbm,
+    routes, gain, dgate, table, index, rw,
+    tok, x2, x3, send, recv, xg, hid, acc, outb, ret, wg, wu, wd, wgo, wuo, wdo, dense, branch, out2,
+    small_sem, index_sem, y_sem, x_sem, out_sem,
     tok_sem, w_sem, wsend_sem, wrecv_sem, d_sem, dsend_sem, drecv_sem,
     send_sem, recv_sem, rsend_sem, rrecv_sem,
 ):
@@ -64,9 +66,29 @@
             lax.rem(z + 8 - dz, 8) * 16 + lax.rem(y + 4 - dy, 4) * 4 + lax.rem(x + 4 - dx, 4)
         )
 
+    small = [
+        pltpu.make_async_copy(a, b, small_sem.at[i])
+        for i, (a, b) in enumerate(
+            ((routes_hbm, routes), (gain_hbm, gain), (rw_hbm, rw), (dgate_hbm, dgate))
+        )
+    ]
     tok_copy = pltpu.make_async_copy(tok_hbm, tok, tok_sem)
+    small[0].start()
     tok_copy.start()
 
+    def greet(sem, device):
+        pl.semaphore_signal(sem, inc=1, device_id=device, device_id_type=MESH)
+
+    barrier = pltpu.get_barrier_semaphore()
+    for d in (4, 3, 5, 2, 6, 1, 7):
+        greet(barrier, (chip(d, 0, 0), tp))
+    for d in (2, 1, 3):
+        greet(barrier, (chip(0, d, 0), tp))
+        greet(barrier, (chip(0, 0, d), tp))
+    greet(barrier, (me, 1 - tp))
+    for copy in small[1:]:
+        copy.start()
+
     @pl.when(tp == 0)
     def _():
         pltpu.make_async_copy(din_hbm, dense.at[0, z, y, x], d_sem).start()
@@ -74,17 +96,6 @@
     @pl.when(tp == 1)
     def _():
         pltpu.make_async_copy(dout_hbm, dense.at[1, z, y, x], d_sem).start()
-
-    barrier = pltpu.get_barrier_semaphore()
-
-    def greet(k, c):
-        pl.semaphore_signal(
-            barrier, inc=1, device_id=(lax.rem(me + k, PEERS), tp), device_id_type=MESH
-        )
-        return c
-
-    lax.fori_loop(1, PEERS, greet, 0)
-    pl.semaphore_signal(barrier, inc=1, device_id=(me, 1 - tp), device_id_type=MESH)
 
     own = [
         pltpu.make_async_copy(a, b, w_sem.at[i])
@@ -98,46 +109,80 @@
         for i, (a, b) in enumerate(((wg_hbm, wgo), (wu_hbm, wuo), (wd_hbm, wdo)))
     ]
 
+    table[...] = jnp.zeros_like(table)
+    small[0].wait()
+    chosen = routes[...]
+    place = place_of(
+        (lax.shift_right_logical(chosen, 4) - z) & 7,
+        ((lax.shift_right_logical(chosen, 2) & 3) - y) & 3,
+        ((chosen & 3) - x) & 3,
+    )
+    sub = lax.broadcasted_iota(jnp.int32, (PEERS, 128), 0)
+    lane = lax.broadcasted_iota(jnp.int32, (PEERS, 128), 1)
+    before = jnp.where(sub < lane, 1.0, 0.0).astype(BF16)
+    token = lax.broadcasted_iota(jnp.int32, (8, 128), 1).astype(F32).astype(BF16)
+    hits, slots = [], []
+    for c in range(2):
+        hit = jnp.where(sub == place[c : c + 1, :], 1.0, 0.0)
+        earlier = jnp.dot(hit.astype(BF16), before, preferred_element_type=F32)
+        if c == 1:
+            earlier = earlier + jnp.sum(hits[0], axis=1, keepdims=True)
+        slot = jnp.sum(hit * earlier, axis=0, keepdims=True)
+        table[3 + c : 4 + c, :] = jnp.clip(
+            place[c : c + 1, :] * CAP + slot.astype(jnp.int32), 0, PEERS * CAP - 1
+        )
+        hits.append(hit)
+        slots.append(slot)
+    for s in range(CAP):
+        held = sum(jnp.where(slots[c] == s, hits[c], 0.0) for c in range(2)).astype(BF16)
+        named = lax.dot_general(
+            token, held, (((1,), (1,)), ((), ())), preferred_element_type=F32
+        )
+        table[s : s + 1, :] = jnp.clip(named[:1].astype(jnp.int32), 0, 127)
+    index_copy = pltpu.make_async_copy(table, index, index_sem)
+    index_copy.start()
+
+    pl.semaphore_wait(barrier, 14)
+    for d in (2, 1, 3):
+        greet(y_sem, (chip(0, d, 0), tp))
+
     tok_copy.wait()
     for copy in own:
         copy.start()
-
+    small[1].wait()
     for i in range(8):
         rows = slice(i * 16, i * 16 + 16)
         wide = tok[rows, :].astype(F32)
         scale = lax.rsqrt(jnp.mean(wide * wide, axis=1, keepdims=True) + NORM_EPS)
-        normed = (wide * scale * gain_ref[...]).astype(BF16)
+        normed = (wide * scale * gain[...]).astype(BF16)
         x2[rows, :] = normed
         x3[rows] = normed.reshape(16, SUB, LANES)
-
     pltpu.make_async_copy(din_hbm, dense.at[tp, z, y, x], d_sem).wait()
-    pl.semaphore_wait(barrier, PEERS)
+    index_copy.wait()
 
     def spread(stage, count, block, target):
-        def one(d, c):
+        for d in range(1, count):
             pltpu.make_async_remote_copy(
                 src_ref=block, dst_ref=block, send_sem=dsend_sem.at[stage],
                 recv_sem=drecv_sem.at[stage], device_id=(target(d), tp), device_id_type=MESH,
             ).start()
-            return c
-
-        lax.fori_loop(1, count, one, 0)
-
-    z_block = dense.at[tp, z, y, x]
-    y_block = dense.at[tp, :, y, x]
-    x_block = dense.at[tp, :, :, x]
+
+    def along_y(d):
+        return chip(0, d, 0)
+
+    def along_x(d):
+        return chip(0, 0, d)
+
     z_all = dense.at[tp, pl.ds(0, 7), y, x]
-    y_all = dense.at[tp, :, pl.ds(0, 3), x]
-    x_all = dense.at[tp, :, :, pl.ds(0, 3)]
+    second_all = dense.at[tp, :, pl.ds(0, 3), x]
+    third_all = dense.at[tp, :, :, pl.ds(0, 3)]
 
     def all_in(ref, sem):
         pltpu.make_async_copy(ref, ref, sem).wait()
 
-    spread(0, 8, z_block, lambda d: chip(d, 0, 0))
-
     def pack(k, c):
         for s in range(CAP):
-            send[k * CAP + s] = x3[src_ref[k * CAP + s]]
+            send[k * CAP + s] = x3[index[s, k]]
         return c
 
     def dispatch(k, c):
@@ -153,28 +198,42 @@
 
         return c
 
-    def pack_and_send(first, last):
-        lax.fori_loop(first, first + PACK, pack, 0)
-
-        def step(b, c):
-            lax.fori_loop(b * PACK + PACK, b * PACK + 2 * PACK, pack, 0)
-            lax.fori_loop(b * PACK, b * PACK + PACK, dispatch, 0)
-            return c
-
-        lax.fori_loop(first // PACK, last // PACK - 1, step, 0)
-        lax.fori_loop(last - PACK, last, dispatch, 0)
-
-    pack_and_send(0, PER_GROUP)
+    lax.fori_loop(0, 32, pack, 0)
+    lax.fori_loop(0, 8, dispatch, 0)
+    spread(0, 8, dense.at[tp, z, y, x], lambda d: chip(d, 0, 0))
+    pl.semaphore_wait(y_sem, 3)
+    for d in (2, 1, 3):
+        greet(x_sem, (chip(0, 0, d), tp))
+    lax.fori_loop(8, 32, dispatch, 0)
+    lax.fori_loop(32, 64, pack, 0)
+    pl.semaphore_wait(x_sem, 3)
+    lax.fori_loop(32, 64, dispatch, 0)
+    lax.fori_loop(64, 128, pack, 0)
     for s in range(CAP):
         recv[SELF * CAP + s] = send[SELF * CAP + s]
 
     all_in(z_all, drecv_sem.at[0])
-    spread(1, 4, y_block, lambda d: chip(0, d, 0))
-    pack_and_send(PER_GROUP, PEERS)
+
+    @pl.when(tp == 0)
+    def _():
+        spread(1, 4, dense.at[0, :, y, x], along_y)
+
+    @pl.when(tp == 1)
+    def _():
+        spread(1, 4, dense.at[1, :, y, x], along_x)
+
+    lax.fori_loop(64, 128, dispatch, 0)
     for copy in other:
         copy.start()
-    all_in(y_all, drecv_sem.at[1])
-    spread(2, 4, x_block, lambda d: chip(0, 0, d))
+    all_in(second_all, drecv_sem.at[1])
+
+    @pl.when(tp == 0)
+    def _():
+        spread(2, 4, dense.at[0, :, :, x], along_x)
+
+    @pl.when(tp == 1)
+    def _():
+        spread(2, 4, dense.at[1, :, y], along_y)
 
     def answer(k, c):
         rows = pl.ds(k * CAP, CAP)
@@ -232,7 +291,7 @@
     for s in range(CAP):
         ret[SELF * CAP + s] = outb[SELF * CAP + s]
 
-    all_in(x_all, drecv_sem.at[2])
+    all_in(third_all, drecv_sem.at[2])
     swap = pltpu.make_async_remote_copy(
         src_ref=dense.at[tp], dst_ref=dense.at[tp], send_sem=dsend_sem.at[3],
         recv_sem=drecv_sem.at[3], device_id=(me, 1 - tp), device_id_type=MESH,
@@ -246,74 +305,65 @@
             x2[:, i * 256 : (i + 1) * 256], dense[0, i].reshape(256, 256), preferred_element_type=F32
         )
     dense_hidden = jax.nn.silu(pre).astype(BF16)
+    small[3].wait()
+    gate = jax.nn.sigmoid(dgate[...])
     for i in range(8):
         part = lax.dot_general(
             dense_hidden, dense[1, i].reshape(256, 256), (((1,), (1,)), ((), ())),
             preferred_element_type=F32,
         )
         for j in range(2):
-            branch[pl.ds(2 * i + j, 128, stride=SUB), :] = part[:, j * LANES : (j + 1) * LANES]
-
-    gate = jax.nn.sigmoid(dgate_ref[...])
+            at = 2 * i + j
+            branch[pl.ds(at, 128, stride=SUB), :] = (
+                part[:, j * LANES : (j + 1) * LANES] * gate[at : at + 1, :]
+            )
+
+    small[2].wait()
     for g in range(GROUPS):
         all_in(ret.at[pl.ds(0, group_bytes(g) * CAP)], rrecv_sem.at[g])
 
-    @pl.loop(0, 128)
-    def _(t):
-        weighted = (
-            rw_ref[2 * t] * ret[pos_ref[2 * t]].astype(F32)
-            + rw_ref[2 * t + 1] * ret[pos_ref[2 * t + 1]].astype(F32)
-        )
+    def combine(t, c):
         tile = pl.ds(pl.multiple_of(t * SUB, SUB), SUB)
-        o_ref[t] = (weighted + gate * branch[tile, :]).astype(BF16)
+        acc[tile, :] = (
+            rw[0, t] * ret[index[3, t]].astype(F32) + rw[1, t] * ret[index[4, t]].astype(F32)
+        ) + branch[tile, :]
+        return c
+
+    for r in range(0, 128, 16):
+        lax.fori_loop(r, r + 16, combine, 0, unroll=8)
+        out2[r : r + 16, :] = (
+            acc[r * SUB : (r + 16) * SUB, :].reshape(16, SUB * LANES).astype(BF16)
+        )
+        pltpu.make_async_copy(out2.at[r : r + 16], o_hbm.at[r : r + 16], out_sem).start()
+    pltpu.make_async_copy(out2, o_hbm, out_sem).wait()
 
     all_in(send.at[pl.ds(0, (PEERS - 1) * CAP)], send_sem)
     all_in(outb.at[pl.ds(0, (PEERS - 1) * CAP)], rsend_sem)
     for copy in other:
         copy.wait_send()
     all_in(z_all, dsend_sem.at[0])
-    all_in(y_all, dsend_sem.at[1])
-    all_in(x_all, dsend_sem.at[2])
+    all_in(second_all, dsend_sem.at[1])
+    all_in(third_all, dsend_sem.at[2])
     swap.wait_send()
-
-
-def tables(routes):
-    rows, top = routes.shape
-    entries = rows * top
-    me = lax.axis_index("ep")
-    flat = routes.reshape(entries)
-    onehot = flat[:, None] == lax.broadcasted_iota(jnp.int32, (1, PEERS), 1)
-    earlier = (
-        lax.broadcasted_iota(jnp.int32, (entries, entries), 0)
-        > lax.broadcasted_iota(jnp.int32, (entries, entries), 1)
-    ).astype(BF16)
-    counted = jnp.dot(earlier, onehot.astype(BF16), preferred_element_type=F32)
-    slot = jnp.sum(jnp.where(onehot, counted, 0.0), axis=1).astype(jnp.int32)
-    dz = (flat // 16 - me // 16) % 8
-    dy = (flat // 4 % 4 - me // 4 % 4) % 4
-    dx = (flat % 4 - me % 4) % 4
-    position = place_of(dz, dy, dx) * CAP + slot
-    places = position[None, :] == lax.broadcasted_iota(jnp.int32, (PEERS * CAP, 1), 0)
-    source = jnp.sum(
-        jnp.where(places, lax.broadcasted_iota(jnp.int32, (1, entries), 1) // top, 0), axis=1
-    )
-    return source, position
 
 
 def shards(
     tokens, norm_gain, routes, route_weights, w_gate, w_up, w_down, dense_in, dense_out, dense_gate
 ):
-    source, position = tables(routes)
-    smem = pl.BlockSpec(memory_space=pltpu.SMEM)
-    vmem = pl.BlockSpec(memory_space=pltpu.VMEM)
     hbm = pl.BlockSpec(memory_space=pl.ANY)
     dma = pltpu.SemaphoreType.DMA
-    out = pl.pallas_call(
+    return pl.pallas_call(
         kernel,
-        out_shape=jax.ShapeDtypeStruct((128, SUB, LANES), BF16),
-        in_specs=[smem, smem, smem, hbm, vmem, vmem, hbm, hbm, hbm, hbm, hbm],
-        out_specs=vmem,
+        out_shape=jax.ShapeDtypeStruct((128, 2048), BF16),
+        in_specs=[hbm] * 10,
+        out_specs=hbm,
         scratch_shapes=[
+            pltpu.VMEM((2, 128), jnp.int32),
+            pltpu.VMEM((1, 2048), F32),
+            pltpu.VMEM((SUB, LANES), F32),
+            pltpu.VMEM((8, 128), jnp.int32),
+            pltpu.SMEM((8, 128), jnp.int32),
+            pltpu.SMEM((2, 128), F32),
             pltpu.VMEM((128, 2048), BF16),
             pltpu.VMEM((128, 2048), BF16),
             pltpu.VMEM((128, SUB, LANES), BF16),
@@ -332,6 +382,8 @@
             pltpu.VMEM((512, 2048), BF16),
             pltpu.VMEM((2, 8, 4, 4, 16, 256), BF16),
             pltpu.VMEM((128 * SUB, LANES), F32),
+            pltpu.VMEM((128, 2048), BF16),
+            dma((4,)), dma, pltpu.SemaphoreType.REGULAR, pltpu.SemaphoreType.REGULAR, dma,
             dma, dma((3,)), dma((3,)), dma((3,)), dma, dma((4,)), dma((4,)),
             dma, dma((GROUPS,)), dma, dma((GROUPS,)),
         ],
@@ -339,10 +391,9 @@
             collective_id=0, has_side_effects=True, vmem_limit_bytes=56 << 20
         ),
     )(
-        source, position, route_weights.reshape(-1), tokens, norm_gain.reshape(1, -1),
+        routes.T, route_weights.T, tokens, norm_gain.reshape(1, -1),
         dense_gate.reshape(SUB, LANES), w_gate[0], w_up[0], w_down[0], dense_in, dense_out,
     )
-    return out.reshape(tokens.shape)
 
 
 def solution(mesh):

time: 93.3 us -> 86.9 us (0.931)
  Pallas kernels: 87.4 us -> 84 us
  local copies, waits for them, and re-layouts: 4.37 us -> 1.88 us
    pallas_call x1, Pallas kernels: 87.4 us -> 84 us  [shards(): pl.pallas_call(kernel, out_shape=jax.ShapeDtypeStruct((128, 2048), BF16),...]
    unnamed x5 -> x1, local copies, waits for them, and re-layouts: 3.54 us -> 1.88 us
where the time goes in v2:
time: 86.9 us; the launch traced here: 85.9 us
  Pallas kernels  84 us (97%)
  local copies, waits for them, and re-layouts  1.88 us (2%)
    pallas_call x1, Pallas kernels, shards(): pl.pallas_call(kernel, out_shape=jax.ShapeDtypeStruct((128, 2048), BF16),...  84 us
    unnamed x1, local copies, waits for them, and re-layouts  1.88 us

profile of v2, /device:TPU:32, one launch (start us, length us, event | category | flops | bytes accessed | tf_op | source)
XLA Modules:
  0.0 85.9 jit_solution(3817286249597749884)
XLA Ops:
  0.0 84.0 %shard_map.100 = bf16[128,2048]{1,0:T(8,128)(2,1)} custom-call(s32[2,128]{1,0:T(2,128)} %bitcast.12, f32[2,128]{1,0:T(2,128)} %bitcast.13, bf16[128,2048]{1,0:T(8,128)(2,1)} %tok_hbm.1, f32[1,2048]{1,0:T(1,128)} %bitcast.10, f32[16,128]{1,0:T(8,128)} %bitcast.11, bf16[2048,512]{1,0:T(8,128)(2,1)} %bitcast.7, bf16[2048,512]{1,0:T(8,128)(2,1)} %bitcast.8, ...), custom_call_target="tpu_custom_call" | custom-call | tf_op jit(solution)/shard_map/pallas_call | solution.py:355
  84.0 1.9 %copy.12 = bf16[128,2048]{1,0:T(8,128)(2,1)} copy(bf16[128,2048]{1,0:T(8,128)(2,1)} %shard_map.100) | data formatting | bytes 1048576

commit v3 on v2

--- a/solution.py
+++ b/solution.py
@@ -45,10 +45,10 @@
 
 def kernel(
     routes_hbm, rw_hbm, tok_hbm, gain_hbm, dgate_hbm, wg_hbm, wu_hbm, wd_hbm, din_hbm, dout_hbm,
-    o_hbm,
+    o_ref,
     routes, gain, dgate, table, index, rw,
-    tok, x2, x3, send, recv, xg, hid, acc, outb, ret, wg, wu, wd, wgo, wuo, wdo, dense, branch, out2,
-    small_sem, index_sem, y_sem, x_sem, out_sem,
+    tok, x2, x3, send, recv, xg, hid, acc, outb, ret, wg, wu, wd, wgo, wuo, wdo, dense, branch,
+    small_sem, index_sem, y_sem, x_sem,
     tok_sem, w_sem, wsend_sem, wrecv_sem, d_sem, dsend_sem, drecv_sem,
     send_sem, recv_sem, rsend_sem, rrecv_sem,
 ):
@@ -111,6 +111,8 @@
 
     table[...] = jnp.zeros_like(table)
     small[0].wait()
+    tok_copy.wait()
+    small[1].wait()
     chosen = routes[...]
     place = place_of(
         (lax.shift_right_logical(chosen, 4) - z) & 7,
@@ -142,14 +144,6 @@
     index_copy = pltpu.make_async_copy(table, index, index_sem)
     index_copy.start()
 
-    pl.semaphore_wait(barrier, 14)
-    for d in (2, 1, 3):
-        greet(y_sem, (chip(0, d, 0), tp))
-
-    tok_copy.wait()
-    for copy in own:
-        copy.start()
-    small[1].wait()
     for i in range(8):
         rows = slice(i * 16, i * 16 + 16)
         wide = tok[rows, :].astype(F32)
@@ -157,6 +151,9 @@
         normed = (wide * scale * gain[...]).astype(BF16)
         x2[rows, :] = normed
         x3[rows] = normed.reshape(16, SUB, LANES)
+    pl.semaphore_wait(barrier, 14)
+    for d in (2, 1, 3):
+        greet(y_sem, (chip(0, d, 0), tp))
     pltpu.make_async_copy(din_hbm, dense.at[tp, z, y, x], d_sem).wait()
     index_copy.wait()
 
@@ -198,17 +195,20 @@
 
         return c
 
-    lax.fori_loop(0, 32, pack, 0)
+    lax.fori_loop(0, 16, pack, 0, unroll=4)
     lax.fori_loop(0, 8, dispatch, 0)
     spread(0, 8, dense.at[tp, z, y, x], lambda d: chip(d, 0, 0))
+    lax.fori_loop(16, 32, pack, 0, unroll=4)
     pl.semaphore_wait(y_sem, 3)
     for d in (2, 1, 3):
         greet(x_sem, (chip(0, 0, d), tp))
     lax.fori_loop(8, 32, dispatch, 0)
-    lax.fori_loop(32, 64, pack, 0)
+    lax.fori_loop(32, 64, pack, 0, unroll=4)
     pl.semaphore_wait(x_sem, 3)
     lax.fori_loop(32, 64, dispatch, 0)
-    lax.fori_loop(64, 128, pack, 0)
+    for copy in own:
+        copy.start()
+    lax.fori_loop(64, 128, pack, 0, unroll=4)
     for s in range(CAP):
         recv[SELF * CAP + s] = send[SELF * CAP + s]
 
@@ -331,11 +331,9 @@
 
     for r in range(0, 128, 16):
         lax.fori_loop(r, r + 16, combine, 0, unroll=8)
-        out2[r : r + 16, :] = (
+        o_ref[r : r + 16, :] = (
             acc[r * SUB : (r + 16) * SUB, :].reshape(16, SUB * LANES).astype(BF16)
         )
-        pltpu.make_async_copy(out2.at[r : r + 16], o_hbm.at[r : r + 16], out_sem).start()
-    pltpu.make_async_copy(out2, o_hbm, out_sem).wait()
 
     all_in(send.at[pl.ds(0, (PEERS - 1) * CAP)], send_sem)
     all_in(outb.at[pl.ds(0, (PEERS - 1) * CAP)], rsend_sem)
@@ -356,7 +354,7 @@
         kernel,
         out_shape=jax.ShapeDtypeStruct((128, 2048), BF16),
         in_specs=[hbm] * 10,
-        out_specs=hbm,
+        out_specs=pl.BlockSpec(memory_space=pltpu.VMEM),
         scratch_shapes=[
             pltpu.VMEM((2, 128), jnp.int32),
             pltpu.VMEM((1, 2048), F32),
@@ -382,17 +380,21 @@
             pltpu.VMEM((512, 2048), BF16),
             pltpu.VMEM((2, 8, 4, 4, 16, 256), BF16),
             pltpu.VMEM((128 * SUB, LANES), F32),
-            pltpu.VMEM((128, 2048), BF16),
-            dma((4,)), dma, pltpu.SemaphoreType.REGULAR, pltpu.SemaphoreType.REGULAR, dma,
+            dma((4,)), dma, pltpu.SemaphoreType.REGULAR, pltpu.SemaphoreType.REGULAR,
             dma, dma((3,)), dma((3,)), dma((3,)), dma, dma((4,)), dma((4,)),
             dma, dma((GROUPS,)), dma, dma((GROUPS,)),
         ],
         compiler_params=pltpu.CompilerParams(
-            collective_id=0, has_side_effects=True, vmem_limit_bytes=56 << 20
+            collective_id=0, has_side_effects=True, vmem_limit_bytes=50 << 20
         ),
     )(
-        routes.T, route_weights.T, tokens, norm_gain.reshape(1, -1),
-        dense_gate.reshape(SUB, LANES), w_gate[0], w_up[0], w_down[0], dense_in, dense_out,
+        *(
+            pltpu.with_memory_space_constraint(operand, pltpu.HBM)
+            for operand in (
+                routes.T, route_weights.T, tokens, norm_gain.reshape(1, -1),
+                dense_gate.reshape(SUB, LANES), w_gate[0], w_up[0], w_down[0], dense_in, dense_out,
+            )
+        )
     )
 
 

time: 86.9 us -> 84.2 us (0.969)
  local copies, waits for them, and re-layouts: 1.88 us -> 0.8 us
    unnamed x1, local copies, waits for them, and re-layouts: 1.88 us -> 0.8 us
where the time goes in v3:
time: 84.2 us; the launch traced here: 84 us
  Pallas kernels  83.2 us (99%)
    pallas_call x1, Pallas kernels, shards(): pl.pallas_call(kernel, out_shape=jax.ShapeDtypeStruct((128, 2048), BF16),...  83.2 us

profile of v3, /device:TPU:32, one launch (start us, length us, event | category | flops | bytes accessed | tf_op | source)
XLA Modules:
  0.0 84.0 jit_solution(4110285227754087750)
XLA Ops:
  0.0 83.2 %shard_map.100 = bf16[128,2048]{1,0:T(8,128)(2,1)S(1)} custom-call(s32[2,128]{1,0:T(2,128)} %bitcast.12, f32[2,128]{1,0:T(2,128)} %bitcast.13, bf16[128,2048]{1,0:T(8,128)(2,1)} %tok_hbm.1, f32[1,2048]{1,0:T(1,128)} %bitcast.10, f32[16,128]{1,0:T(8,128)} %bitcast.11, bf16[2048,512]{1,0:T(8,128)(2,1)} %bitcast.7, bf16[2048,512]{1,0:T(8,128)(2,1)} %bitcast.8, ...), custom_call_target="tpu_custom_call" | custom-call | tf_op jit(solution)/shard_map/pallas_call | solution.py:353
  83.2 0.8 copy.12

commit v4 on v3

--- a/solution.py
+++ b/solution.py
@@ -20,7 +20,8 @@
 GROUPS = 2
 PER_GROUP = PEERS // GROUPS
 ROWS = PER_GROUP * CAP
-PACK = 16
+LOCAL = 3
+DZ = (4, 5, 3, 6, 2, 7, 1, 0)
 
 
 def place_of(dz, dy, dx):
@@ -46,9 +47,9 @@
 def kernel(
     routes_hbm, rw_hbm, tok_hbm, gain_hbm, dgate_hbm, wg_hbm, wu_hbm, wd_hbm, din_hbm, dout_hbm,
     o_ref,
-    routes, gain, dgate, table, index, rw,
+    routes, gain, dgate, table, index, rw, xn, tn, indexn,
     tok, x2, x3, send, recv, xg, hid, acc, outb, ret, wg, wu, wd, wgo, wuo, wdo, dense, branch,
-    small_sem, index_sem, y_sem, x_sem,
+    small_sem, index_sem, y_sem, x_sem, nsend_sem, nrecv_sem, tsend_sem, trecv_sem, indexn_sem,
     tok_sem, w_sem, wsend_sem, wrecv_sem, d_sem, dsend_sem, drecv_sem,
     send_sem, recv_sem, rsend_sem, rrecv_sem,
 ):
@@ -152,6 +153,18 @@
         x2[rows, :] = normed
         x3[rows] = normed.reshape(16, SUB, LANES)
     pl.semaphore_wait(barrier, 14)
+    ahead = [
+        pltpu.make_async_remote_copy(
+            src_ref=a, dst_ref=b.at[i], send_sem=ss.at[i], recv_sem=rs.at[i],
+            device_id=(chip(d, 0, 0), tp), device_id_type=MESH,
+        )
+        for a, b, ss, rs in (
+            (table, tn, tsend_sem, trecv_sem), (x3, xn, nsend_sem, nrecv_sem)
+        )
+        for i, d in enumerate((1, 7))
+    ]
+    for copy in ahead:
+        copy.start()
     for d in (2, 1, 3):
         greet(y_sem, (chip(0, d, 0), tp))
     pltpu.make_async_copy(din_hbm, dense.at[tp, z, y, x], d_sem).wait()
@@ -177,54 +190,93 @@
     def all_in(ref, sem):
         pltpu.make_async_copy(ref, ref, sem).wait()
 
-    def pack(k, c):
+    def pack(k, rows_of, index_of):
         for s in range(CAP):
-            send[k * CAP + s] = x3[index[s, k]]
-        return c
-
-    def dispatch(k, c):
+            send[k * CAP + s] = rows_of[index_of[s, k]]
+
+    def dispatch(k, z_to, r):
         rows = pl.ds(k * CAP, CAP)
-
-        @pl.when(k != SELF)
-        def _():
-            pltpu.make_async_remote_copy(
-                src_ref=send.at[rows], dst_ref=recv.at[rows], send_sem=send_sem,
-                recv_sem=recv_sem.at[lax.div(k, PER_GROUP)],
-                device_id=(chip(*offset_of(k)), tp), device_id_type=MESH,
-            ).start()
-
-        return c
-
-    lax.fori_loop(0, 16, pack, 0, unroll=4)
-    lax.fori_loop(0, 8, dispatch, 0)
+        device = z_to * 16 + lax.rem(y + lax.rem(r, 4), 4) * 4 + lax.rem(x + lax.div(r, 4), 4)
+        pltpu.make_async_remote_copy(
+            src_ref=send.at[rows], dst_ref=recv.at[rows], send_sem=send_sem,
+            recv_sem=recv_sem.at[lax.div(k, PER_GROUP)],
+            device_id=(device, tp), device_id_type=MESH,
+        ).start()
+
+    for r in range(4):
+        pack(r * 8, x3, index)
     spread(0, 8, dense.at[tp, z, y, x], lambda d: chip(d, 0, 0))
-    lax.fori_loop(16, 32, pack, 0, unroll=4)
     pl.semaphore_wait(y_sem, 3)
     for d in (2, 1, 3):
         greet(x_sem, (chip(0, 0, d), tp))
-    lax.fori_loop(8, 32, dispatch, 0)
-    lax.fori_loop(32, 64, pack, 0, unroll=4)
+    for r in range(4):
+        dispatch(r * 8, lax.rem(z + 4, 8), r)
+
+    def pack_flat(r, c):
+        pack(r * 8 + 7, x3, index)
+        return c
+
+    def dispatch_flat(r, c):
+        dispatch(r * 8 + 7, z, r)
+        return c
+
+    lax.fori_loop(0, 16, pack_flat, 0)
     pl.semaphore_wait(x_sem, 3)
-    lax.fori_loop(32, 64, dispatch, 0)
+    lax.fori_loop(1, 16, dispatch_flat, 0)
     for copy in own:
         copy.start()
-    lax.fori_loop(64, 128, pack, 0, unroll=4)
-    for s in range(CAP):
-        recv[SELF * CAP + s] = send[SELF * CAP + s]
-
-    all_in(z_all, drecv_sem.at[0])
-
-    @pl.when(tp == 0)
-    def _():
-        spread(1, 4, dense.at[0, :, y, x], along_y)
-
-    @pl.when(tp == 1)
-    def _():
-        spread(1, 4, dense.at[1, :, y, x], along_x)
-
-    lax.fori_loop(64, 128, dispatch, 0)
     for copy in other:
         copy.start()
+
+    onward = []
+    for i in range(2):
+        ahead[i].wait_recv()
+        onward.append(pltpu.make_async_copy(tn.at[i], indexn.at[i], indexn_sem.at[i]))
+        onward[i].start()
+    for i in range(2):
+        onward[i].wait()
+    for i in range(2):
+        ahead[2 + i].wait_recv()
+
+    def relay_pair(h, c):
+        def each(visit):
+            for p in range(2):
+                r = 2 * h + p
+                for at in range(7):
+                    if at == 0:
+                        pl.when(h >= 2)(lambda r=r, p=p: visit(r, 0, p, False))
+                    else:
+                        visit(r, at, at % 2, p == 0 and at >= 5)
+
+        def do_pack(r, at, i, local):
+            pack(r * 8 + at, xn.at[i], indexn.at[i])
+
+        def do_send(r, at, i, local):
+            z_to = lax.rem(z + (7 if i == 0 else 1) + DZ[at], 8)
+            if local:
+                pl.when(h > 0)(lambda: dispatch(r * 8 + at, z_to, r))
+            else:
+                dispatch(r * 8 + at, z_to, r)
+
+        each(do_pack)
+        each(do_send)
+        return c
+
+    lax.fori_loop(0, 4, relay_pair, 0)
+    for s in range(LOCAL * CAP):
+        recv[5 * CAP + s] = send[5 * CAP + s]
+
+    all_in(z_all, drecv_sem.at[0])
+
+    @pl.when(tp == 0)
+    def _():
+        spread(1, 4, dense.at[0, :, y, x], along_y)
+
+    @pl.when(tp == 1)
+    def _():
+        spread(1, 4, dense.at[1, :, y, x], along_x)
+
+    lax.fori_loop(4, 8, relay_pair, 0)
     all_in(second_all, drecv_sem.at[1])
 
     @pl.when(tp == 0)
@@ -253,7 +305,7 @@
 
     for g in range(GROUPS):
         base = g * ROWS
-        all_in(recv.at[pl.ds(0, group_bytes(g) * CAP)], recv_sem.at[g])
+        all_in(recv.at[pl.ds(0, (PER_GROUP - LOCAL * (g == 0)) * CAP)], recv_sem.at[g])
 
         for r in range(0, ROWS, 16):
             xg[r : r + 16, :] = recv[base + r : base + r + 16].reshape(16, SUB * LANES)
@@ -335,7 +387,9 @@
             acc[r * SUB : (r + 16) * SUB, :].reshape(16, SUB * LANES).astype(BF16)
         )
 
-    all_in(send.at[pl.ds(0, (PEERS - 1) * CAP)], send_sem)
+    all_in(send.at[pl.ds(0, (PEERS - LOCAL) * CAP)], send_sem)
+    for copy in ahead:
+        copy.wait_send()
     all_in(outb.at[pl.ds(0, (PEERS - 1) * CAP)], rsend_sem)
     for copy in other:
         copy.wait_send()
@@ -362,6 +416,9 @@
             pltpu.VMEM((8, 128), jnp.int32),
             pltpu.SMEM((8, 128), jnp.int32),
             pltpu.SMEM((2, 128), F32),
+            pltpu.VMEM((2, 128, SUB, LANES), BF16),
+            pltpu.VMEM((2, 8, 128), jnp.int32),
+            pltpu.SMEM((2, 8, 128), jnp.int32),
             pltpu.VMEM((128, 2048), BF16),
             pltpu.VMEM((128, 2048), BF16),
             pltpu.VMEM((128, SUB, LANES), BF16),
@@ -381,6 +438,7 @@
             pltpu.VMEM((2, 8, 4, 4, 16, 256), BF16),
             pltpu.VMEM((128 * SUB, LANES), F32),
             dma((4,)), dma, pltpu.SemaphoreType.REGULAR, pltpu.SemaphoreType.REGULAR,
+            dma((2,)), dma((2,)), dma((2,)), dma((2,)), dma((2,)),
             dma, dma((3,)), dma((3,)), dma((3,)), dma, dma((4,)), dma((4,)),
             dma, dma((GROUPS,)), dma, dma((GROUPS,)),
         ],

time: 84.2 us -> 81 us (0.962)
  Pallas kernels: 83.2 us -> 80.1 us
    pallas_call x1, Pallas kernels: 83.2 us -> 80.1 us  [shards(): pl.pallas_call(kernel, out_shape=jax.ShapeDtypeStruct((128, 2048), BF16),...]
where the time goes in v4:
time: 81 us; the launch traced here: 80.9 us
  Pallas kernels  80.1 us (99%)
    pallas_call x1, Pallas kernels, shards(): pl.pallas_call(kernel, out_shape=jax.ShapeDtypeStruct((128, 2048), BF16),...  80.1 us

profile of v4, /device:TPU:32, one launch (start us, length us, event | category | flops | bytes accessed | tf_op | source)
XLA Modules:
  0.0 80.9 jit_solution(18197789595425654588)
XLA Ops:
  0.0 80.1 %shard_map.100 = bf16[128,2048]{1,0:T(8,128)(2,1)S(1)} custom-call(s32[2,128]{1,0:T(2,128)} %bitcast.12, f32[2,128]{1,0:T(2,128)} %bitcast.13, bf16[128,2048]{1,0:T(8,128)(2,1)} %tok_hbm.1, f32[1,2048]{1,0:T(1,128)} %bitcast.10, f32[16,128]{1,0:T(8,128)} %bitcast.11, bf16[2048,512]{1,0:T(8,128)(2,1)} %bitcast.7, bf16[2048,512]{1,0:T(8,128)(2,1)} %bitcast.8, ...), custom_call_target="tpu_custom_call" | custom-call | tf_op jit(solution)/shard_map/pallas_call | solution.py:407
  80.1 0.8 copy.12

commit v5 on v4

--- a/solution.py
+++ b/solution.py
@@ -17,10 +17,11 @@
 LANES = 128
 SUB = 16
 SELF = 7
-GROUPS = 2
+GROUPS = 4
 PER_GROUP = PEERS // GROUPS
 ROWS = PER_GROUP * CAP
 LOCAL = 3
+CHUNK = 16
 DZ = (4, 5, 3, 6, 2, 7, 1, 0)
 
 
@@ -47,9 +48,9 @@
 def kernel(
     routes_hbm, rw_hbm, tok_hbm, gain_hbm, dgate_hbm, wg_hbm, wu_hbm, wd_hbm, din_hbm, dout_hbm,
     o_ref,
-    routes, gain, dgate, table, index, rw, xn, tn, indexn,
+    routes, gain, dgate, table, index, rw, xn, tn, indexn, share, sharen, part, pn, weight, weightn,
     tok, x2, x3, send, recv, xg, hid, acc, outb, ret, wg, wu, wd, wgo, wuo, wdo, dense, branch,
-    small_sem, index_sem, y_sem, x_sem, nsend_sem, nrecv_sem, tsend_sem, trecv_sem, indexn_sem,
+    small_sem, index_sem, y_sem, x_sem, nsend_sem, nrecv_sem, tsend_sem, trecv_sem, indexn_sem, ssend_sem, srecv_sem, weight_sem, weightn_sem, psend_sem, precv_sem,
     tok_sem, w_sem, wsend_sem, wrecv_sem, d_sem, dsend_sem, drecv_sem,
     send_sem, recv_sem, rsend_sem, rrecv_sem,
 ):
@@ -145,6 +146,19 @@
     index_copy = pltpu.make_async_copy(table, index, index_sem)
     index_copy.start()
 
+    small[2].wait()
+    at = place & 7
+    flank = (at == 0) & (place >= 32)
+    even = (lax.shift_right_logical(place, 3) & 1) == 0
+    up = ((at == 2) | (at == 4) | (at == 6)) | (flank & even)
+    down = ((at == 1) | (at == 3) | (at == 5)) | (flank & ~even)
+    share[...] = jnp.zeros_like(share)
+    share[0:2, :] = jnp.where(up, rw[...], 0.0)
+    share[2:4, :] = jnp.where(down, rw[...], 0.0)
+    share[4:6, :] = jnp.where(up | down, 0.0, rw[...])
+    weight_copy = pltpu.make_async_copy(share, weight, weight_sem)
+    weight_copy.start()
+
     for i in range(8):
         rows = slice(i * 16, i * 16 + 16)
         wide = tok[rows, :].astype(F32)
@@ -152,14 +166,37 @@
         normed = (wide * scale * gain[...]).astype(BF16)
         x2[rows, :] = normed
         x3[rows] = normed.reshape(16, SUB, LANES)
+    def spread(stage, count, block, target):
+        for d in range(1, count):
+            pltpu.make_async_remote_copy(
+                src_ref=block, dst_ref=block, send_sem=dsend_sem.at[stage],
+                recv_sem=drecv_sem.at[stage], device_id=(target(d), tp), device_id_type=MESH,
+            ).start()
+
+    def along_y(d):
+        return chip(0, d, 0)
+
+    def along_x(d):
+        return chip(0, 0, d)
+
+    z_all = dense.at[tp, pl.ds(0, 7), y, x]
+    second_all = dense.at[tp, :, pl.ds(0, 3), x]
+    third_all = dense.at[tp, :, :, pl.ds(0, 3)]
+
+    def all_in(ref, sem):
+        pltpu.make_async_copy(ref, ref, sem).wait()
+
+    pltpu.make_async_copy(din_hbm, dense.at[tp, z, y, x], d_sem).wait()
     pl.semaphore_wait(barrier, 14)
+    spread(0, 8, dense.at[tp, z, y, x], lambda d: chip(d, 0, 0))
     ahead = [
         pltpu.make_async_remote_copy(
             src_ref=a, dst_ref=b.at[i], send_sem=ss.at[i], recv_sem=rs.at[i],
             device_id=(chip(d, 0, 0), tp), device_id_type=MESH,
         )
         for a, b, ss, rs in (
-            (table, tn, tsend_sem, trecv_sem), (x3, xn, nsend_sem, nrecv_sem)
+            (table, tn, tsend_sem, trecv_sem), (x3, xn, nsend_sem, nrecv_sem),
+            (share, sharen, ssend_sem, srecv_sem),
         )
         for i, d in enumerate((1, 7))
     ]
@@ -167,28 +204,7 @@
         copy.start()
     for d in (2, 1, 3):
         greet(y_sem, (chip(0, d, 0), tp))
-    pltpu.make_async_copy(din_hbm, dense.at[tp, z, y, x], d_sem).wait()
     index_copy.wait()
-
-    def spread(stage, count, block, target):
-        for d in range(1, count):
-            pltpu.make_async_remote_copy(
-                src_ref=block, dst_ref=block, send_sem=dsend_sem.at[stage],
-                recv_sem=drecv_sem.at[stage], device_id=(target(d), tp), device_id_type=MESH,
-            ).start()
-
-    def along_y(d):
-        return chip(0, d, 0)
-
-    def along_x(d):
-        return chip(0, 0, d)
-
-    z_all = dense.at[tp, pl.ds(0, 7), y, x]
-    second_all = dense.at[tp, :, pl.ds(0, 3), x]
-    third_all = dense.at[tp, :, :, pl.ds(0, 3)]
-
-    def all_in(ref, sem):
-        pltpu.make_async_copy(ref, ref, sem).wait()
 
     def pack(k, rows_of, index_of):
         for s in range(CAP):
@@ -205,7 +221,6 @@
 
     for r in range(4):
         pack(r * 8, x3, index)
-    spread(0, 8, dense.at[tp, z, y, x], lambda d: chip(d, 0, 0))
     pl.semaphore_wait(y_sem, 3)
     for d in (2, 1, 3):
         greet(x_sem, (chip(0, 0, d), tp))
@@ -227,6 +242,26 @@
         copy.start()
     for copy in other:
         copy.start()
+
+    all_in(z_all, drecv_sem.at[0])
+
+    @pl.when(tp == 0)
+    def _():
+        spread(1, 4, dense.at[0, :, y, x], along_y)
+
+    @pl.when(tp == 1)
+    def _():
+        spread(1, 4, dense.at[1, :, y, x], along_x)
+
+    all_in(second_all, drecv_sem.at[1])
+
+    @pl.when(tp == 0)
+    def _():
+        spread(2, 4, dense.at[0, :, :, x], along_x)
+
+    @pl.when(tp == 1)
+    def _():
+        spread(2, 4, dense.at[1, :, y], along_y)
 
     onward = []
     for i in range(2):
@@ -266,42 +301,33 @@
     for s in range(LOCAL * CAP):
         recv[5 * CAP + s] = send[5 * CAP + s]
 
-    all_in(z_all, drecv_sem.at[0])
-
-    @pl.when(tp == 0)
-    def _():
-        spread(1, 4, dense.at[0, :, y, x], along_y)
-
-    @pl.when(tp == 1)
-    def _():
-        spread(1, 4, dense.at[1, :, y, x], along_x)
-
     lax.fori_loop(4, 8, relay_pair, 0)
-    all_in(second_all, drecv_sem.at[1])
-
-    @pl.when(tp == 0)
-    def _():
-        spread(2, 4, dense.at[0, :, :, x], along_x)
-
-    @pl.when(tp == 1)
-    def _():
-        spread(2, 4, dense.at[1, :, y], along_y)
-
-    def answer(k, c):
+    def answer(k, z_to, r, sem):
         rows = pl.ds(k * CAP, CAP)
-
-        @pl.when(k != SELF)
-        def _():
-            pltpu.make_async_remote_copy(
-                src_ref=outb.at[rows], dst_ref=ret.at[rows], send_sem=rsend_sem,
-                recv_sem=rrecv_sem.at[lax.div(k, PER_GROUP)],
-                device_id=(back(*offset_of(k)), tp), device_id_type=MESH,
-            ).start()
-
-        return c
-
-    def group_bytes(g):
-        return PER_GROUP - 1 if g == 0 else PER_GROUP
+        device = (
+            lax.rem(z_to, 8) * 16 + lax.rem(y + 4 - lax.rem(r, 4), 4) * 4
+            + lax.rem(x + 4 - lax.div(r, 4), 4)
+        )
+        pltpu.make_async_remote_copy(
+            src_ref=outb.at[rows], dst_ref=ret.at[rows], send_sem=rsend_sem,
+            recv_sem=rrecv_sem.at[sem], device_id=(device, tp), device_id_type=MESH,
+        ).start()
+
+    def answers(g):
+        def one(r, c):
+            @pl.when(r >= 4)
+            def _():
+                answer(r * 8, z + 13 - 2 * lax.rem(r, 2), r, g)
+
+            for at in range(1, 8):
+                z_to = z + 8 - DZ[at] + (0 if at == 7 else 1 - 2 * (at % 2))
+                if at >= 5 and g == 0:
+                    pl.when(r > 0)(lambda at=at, z_to=z_to: answer(r * 8 + at, z_to, r, g))
+                else:
+                    answer(r * 8 + at, z_to, r, g)
+            return c
+
+        lax.fori_loop(g * 16 // GROUPS, (g + 1) * 16 // GROUPS, one, 0)
 
     for g in range(GROUPS):
         base = g * ROWS
@@ -338,10 +364,46 @@
                 acc[r * SUB : (r + 16) * SUB, :].reshape(16, SUB, LANES).astype(BF16)
             )
 
-        lax.fori_loop(g * PER_GROUP, (g + 1) * PER_GROUP, answer, 0)
-
-    for s in range(CAP):
-        ret[SELF * CAP + s] = outb[SELF * CAP + s]
+        answers(g)
+        for r in range(4 if g == 0 else 0):
+            answer(r * 8, z + 4, r, GROUPS)
+    for s in range(LOCAL * CAP):
+        ret[5 * CAP + s] = outb[5 * CAP + s]
+
+    for i in range(2):
+        ahead[4 + i].wait_recv()
+        copy = pltpu.make_async_copy(sharen.at[i], weightn.at[i], weightn_sem.at[i])
+        copy.start()
+        copy.wait()
+    all_in(ret.at[pl.ds(0, (PER_GROUP - LOCAL - 4) * CAP)], rrecv_sem.at[0])
+    all_in(ret.at[pl.ds(0, 4 * CAP)], rrecv_sem.at[GROUPS])
+    for g in range(1, GROUPS):
+        all_in(ret.at[pl.ds(0, PER_GROUP * CAP)], rrecv_sem.at[g])
+
+    def chosen_rows(t, index_of, weight_of, first):
+        return weight_of[first, t] * ret[index_of[3, t]].astype(F32) + weight_of[
+            first + 1, t
+        ] * ret[index_of[4, t]].astype(F32)
+
+    def send_part(j):
+        rows = slice(j * CHUNK, (j + 1) * CHUNK)
+        for i, d in enumerate((7, 1)):
+            pltpu.make_async_remote_copy(
+                src_ref=part.at[i, rows], dst_ref=pn.at[i, rows], send_sem=psend_sem.at[i],
+                recv_sem=precv_sem.at[i, j], device_id=(chip(d, 0, 0), tp), device_id_type=MESH,
+            ).start()
+
+    def relay_sums(t, c):
+        for i in range(2):
+            part[i, t] = chosen_rows(t, indexn.at[i], weightn.at[i], 2 * i).astype(BF16)
+        return c
+
+    chunks = 128 // CHUNK
+    for j in range(chunks):
+        lax.fori_loop(j * CHUNK, (j + 1) * CHUNK, relay_sums, 0, unroll=4)
+        if j > 0:
+            send_part(j - 1)
+    send_part(chunks - 1)
 
     all_in(third_all, drecv_sem.at[2])
     swap = pltpu.make_async_remote_copy(
@@ -360,37 +422,40 @@
     small[3].wait()
     gate = jax.nn.sigmoid(dgate[...])
     for i in range(8):
-        part = lax.dot_general(
+        piece = lax.dot_general(
             dense_hidden, dense[1, i].reshape(256, 256), (((1,), (1,)), ((), ())),
             preferred_element_type=F32,
         )
         for j in range(2):
             at = 2 * i + j
             branch[pl.ds(at, 128, stride=SUB), :] = (
-                part[:, j * LANES : (j + 1) * LANES] * gate[at : at + 1, :]
+                piece[:, j * LANES : (j + 1) * LANES] * gate[at : at + 1, :]
             )
 
-    small[2].wait()
-    for g in range(GROUPS):
-        all_in(ret.at[pl.ds(0, group_bytes(g) * CAP)], rrecv_sem.at[g])
-
-    def combine(t, c):
+    weight_copy.wait()
+
+    def straight(t, c):
         tile = pl.ds(pl.multiple_of(t * SUB, SUB), SUB)
-        acc[tile, :] = (
-            rw[0, t] * ret[index[3, t]].astype(F32) + rw[1, t] * ret[index[4, t]].astype(F32)
-        ) + branch[tile, :]
+        acc[tile, :] = chosen_rows(t, index, weight, 4) + branch[tile, :]
         return c
 
-    for r in range(0, 128, 16):
-        lax.fori_loop(r, r + 16, combine, 0, unroll=8)
-        o_ref[r : r + 16, :] = (
-            acc[r * SUB : (r + 16) * SUB, :].reshape(16, SUB * LANES).astype(BF16)
-        )
+    lax.fori_loop(0, 128, straight, 0, unroll=4)
+    for j in range(chunks):
+        rows = slice(j * CHUNK, (j + 1) * CHUNK)
+        for i in range(2):
+            all_in(pn.at[i, rows], precv_sem.at[i, j])
+        total = (
+            acc[j * CHUNK * SUB : (j + 1) * CHUNK * SUB, :].reshape(CHUNK, SUB, LANES)
+            + pn[0, rows].astype(F32) + pn[1, rows].astype(F32)
+        )
+        o_ref[rows, :] = total.reshape(CHUNK, SUB * LANES).astype(BF16)
 
     all_in(send.at[pl.ds(0, (PEERS - LOCAL) * CAP)], send_sem)
     for copy in ahead:
         copy.wait_send()
-    all_in(outb.at[pl.ds(0, (PEERS - 1) * CAP)], rsend_sem)
+    all_in(outb.at[pl.ds(0, (PEERS - LOCAL) * CAP)], rsend_sem)
+    for i in range(2):
+        all_in(part.at[i], psend_sem.at[i])
     for copy in other:
         copy.wait_send()
     all_in(z_all, dsend_sem.at[0])
@@ -415,10 +480,16 @@
             pltpu.VMEM((SUB, LANES), F32),
             pltpu.VMEM((8, 128), jnp.int32),
             pltpu.SMEM((8, 128), jnp.int32),
-            pltpu.SMEM((2, 128), F32),
+            pltpu.VMEM((2, 128), F32),
             pltpu.VMEM((2, 128, SUB, LANES), BF16),
             pltpu.VMEM((2, 8, 128), jnp.int32),
             pltpu.SMEM((2, 8, 128), jnp.int32),
+            pltpu.VMEM((8, 128), F32),
+            pltpu.VMEM((2, 8, 128), F32),
+            pltpu.VMEM((2, 128, SUB, LANES), BF16),
+            pltpu.VMEM((2, 128, SUB, LANES), BF16),
+            pltpu.SMEM((8, 128), F32),
+            pltpu.SMEM((2, 8, 128), F32),
             pltpu.VMEM((128, 2048), BF16),
             pltpu.VMEM((128, 2048), BF16),
             pltpu.VMEM((128, SUB, LANES), BF16),
@@ -426,7 +497,7 @@
             pltpu.VMEM((PEERS * CAP, SUB, LANES), BF16),
             pltpu.VMEM((ROWS, 2048), BF16),
             pltpu.VMEM((ROWS, 1024), BF16),
-            pltpu.VMEM((ROWS * SUB, LANES), F32),
+            pltpu.VMEM((2048, LANES) if ROWS < 128 else (ROWS * SUB, LANES), F32),
             pltpu.VMEM((PEERS * CAP, SUB, LANES), BF16),
             pltpu.VMEM((PEERS * CAP, SUB, LANES), BF16),
             pltpu.VMEM((2048, 512), BF16),
@@ -439,8 +510,9 @@
             pltpu.VMEM((128 * SUB, LANES), F32),
             dma((4,)), dma, pltpu.SemaphoreType.REGULAR, pltpu.SemaphoreType.REGULAR,
             dma((2,)), dma((2,)), dma((2,)), dma((2,)), dma((2,)),
+            dma((2,)), dma((2,)), dma, dma((2,)), dma((2,)), dma((2, 128 // CHUNK)),
             dma, dma((3,)), dma((3,)), dma((3,)), dma, dma((4,)), dma((4,)),
-            dma, dma((GROUPS,)), dma, dma((GROUPS,)),
+            dma, dma((GROUPS,)), dma, dma((GROUPS + 1,)),
         ],
         compiler_params=pltpu.CompilerParams(
             collective_id=0, has_side_effects=True, vmem_limit_bytes=50 << 20

time: 81 us -> 80.6 us (level); the launches traced: 80.9 us -> 79.2 us
  Pallas kernels: 80.1 us -> 78.4 us
    pallas_call x1, Pallas kernels: 80.1 us -> 78.4 us  [shards(): pl.pallas_call(kernel, out_shape=jax.ShapeDtypeStruct((128, 2048), BF16),...]
where the time goes in v5:
time: 80.6 us; the launch traced here: 79.2 us
  Pallas kernels  78.4 us (97%)
    pallas_call x1, Pallas kernels, shards(): pl.pallas_call(kernel, out_shape=jax.ShapeDtypeStruct((128, 2048), BF16),...  78.4 us

profile of v5, /device:TPU:32, one launch (start us, length us, event | category | flops | bytes accessed | tf_op | source)
XLA Modules:
  0.0 79.2 jit_solution(10845347581287372449)
XLA Ops:
  0.0 78.4 %shard_map.100 = bf16[128,2048]{1,0:T(8,128)(2,1)S(1)} custom-call(s32[2,128]{1,0:T(2,128)} %bitcast.12, f32[2,128]{1,0:T(2,128)} %bitcast.13, bf16[128,2048]{1,0:T(8,128)(2,1)} %tok_hbm.1, f32[1,2048]{1,0:T(1,128)} %bitcast.10, f32[16,128]{1,0:T(8,128)} %bitcast.11, bf16[2048,512]{1,0:T(8,128)(2,1)} %bitcast.7, bf16[2048,512]{1,0:T(8,128)(2,1)} %bitcast.8, ...), custom_call_target="tpu_custom_call" | custom-call | tf_op jit(solution)/shard_map/pallas_call | solution.py:472
  78.4 0.8 %copy.12 = bf16[128,2048]{1,0:T(8,128)(2,1)} copy(bf16[128,2048]{1,0:T(8,128)(2,1)S(1)} %shard_map.100) | data formatting | bytes 1048576

commit v6 on v5

--- a/solution.py
+++ b/solution.py
@@ -48,7 +48,7 @@
 def kernel(
     routes_hbm, rw_hbm, tok_hbm, gain_hbm, dgate_hbm, wg_hbm, wu_hbm, wd_hbm, din_hbm, dout_hbm,
     o_ref,
-    routes, gain, dgate, table, index, rw, xn, tn, indexn, share, sharen, part, pn, weight, weightn,
+    routes, gain, dgate, table, index, rw, far, xn, tn, indexn, share, sharen, part, pn, weight, weightn,
     tok, x2, x3, send, recv, xg, hid, acc, outb, ret, wg, wu, wd, wgo, wuo, wdo, dense, branch,
     small_sem, index_sem, y_sem, x_sem, nsend_sem, nrecv_sem, tsend_sem, trecv_sem, indexn_sem, ssend_sem, srecv_sem, weight_sem, weightn_sem, psend_sem, precv_sem,
     tok_sem, w_sem, wsend_sem, wrecv_sem, d_sem, dsend_sem, drecv_sem,
@@ -77,6 +77,10 @@
     tok_copy = pltpu.make_async_copy(tok_hbm, tok, tok_sem)
     small[0].start()
     tok_copy.start()
+
+    for r in range(4):
+        for s in range(CAP):
+            ret[r * 8 * CAP + s] = jnp.zeros((SUB, LANES), BF16)
 
     def greet(sem, device):
         pl.semaphore_signal(sem, inc=1, device_id=device, device_id_type=MESH)
@@ -135,6 +139,10 @@
         table[3 + c : 4 + c, :] = jnp.clip(
             place[c : c + 1, :] * CAP + slot.astype(jnp.int32), 0, PEERS * CAP - 1
         )
+        table[5 + c : 6 + c, :] = jnp.clip(
+            lax.shift_right_logical(place[c : c + 1, :], 3) * CAP + slot.astype(jnp.int32),
+            0, 4 * CAP - 1,
+        )
         hits.append(hit)
         slots.append(slot)
     for s in range(CAP):
@@ -155,7 +163,8 @@
     share[...] = jnp.zeros_like(share)
     share[0:2, :] = jnp.where(up, rw[...], 0.0)
     share[2:4, :] = jnp.where(down, rw[...], 0.0)
-    share[4:6, :] = jnp.where(up | down, 0.0, rw[...])
+    share[4:6, :] = jnp.where(at == 7, rw[...], 0.0)
+    share[6:8, :] = jnp.where((at == 0) & (place < 32), rw[...], 0.0)
     weight_copy = pltpu.make_async_copy(share, weight, weight_sem)
     weight_copy.start()
 
@@ -302,14 +311,14 @@
         recv[5 * CAP + s] = send[5 * CAP + s]
 
     lax.fori_loop(4, 8, relay_pair, 0)
-    def answer(k, z_to, r, sem):
+    def answer(k, z_to, r, sem, into=None):
         rows = pl.ds(k * CAP, CAP)
         device = (
             lax.rem(z_to, 8) * 16 + lax.rem(y + 4 - lax.rem(r, 4), 4) * 4
             + lax.rem(x + 4 - lax.div(r, 4), 4)
         )
         pltpu.make_async_remote_copy(
-            src_ref=outb.at[rows], dst_ref=ret.at[rows], send_sem=rsend_sem,
+            src_ref=outb.at[rows], dst_ref=ret.at[rows] if into is None else into, send_sem=rsend_sem,
             recv_sem=rrecv_sem.at[sem], device_id=(device, tp), device_id_type=MESH,
         ).start()
 
@@ -365,8 +374,8 @@
             )
 
         answers(g)
-        for r in range(4 if g == 0 else 0):
-            answer(r * 8, z + 4, r, GROUPS)
+    for r in range(4):
+        answer(r * 8, z + 4, r, GROUPS, far.at[pl.ds(r * CAP, CAP)])
     for s in range(LOCAL * CAP):
         ret[5 * CAP + s] = outb[5 * CAP + s]
 
@@ -376,7 +385,6 @@
         copy.start()
         copy.wait()
     all_in(ret.at[pl.ds(0, (PER_GROUP - LOCAL - 4) * CAP)], rrecv_sem.at[0])
-    all_in(ret.at[pl.ds(0, 4 * CAP)], rrecv_sem.at[GROUPS])
     for g in range(1, GROUPS):
         all_in(ret.at[pl.ds(0, PER_GROUP * CAP)], rrecv_sem.at[g])
 
@@ -433,10 +441,14 @@
             )
 
     weight_copy.wait()
+    all_in(far, rrecv_sem.at[GROUPS])
 
     def straight(t, c):
         tile = pl.ds(pl.multiple_of(t * SUB, SUB), SUB)
-        acc[tile, :] = chosen_rows(t, index, weight, 4) + branch[tile, :]
+        from_far = weight[6, t] * far[index[5, t]].astype(F32) + weight[7, t] * far[
+            index[6, t]
+        ].astype(F32)
+        acc[tile, :] = chosen_rows(t, index, weight, 4) + from_far + branch[tile, :]
         return c
 
     lax.fori_loop(0, 128, straight, 0, unroll=4)
@@ -481,6 +493,7 @@
             pltpu.VMEM((8, 128), jnp.int32),
             pltpu.SMEM((8, 128), jnp.int32),
             pltpu.VMEM((2, 128), F32),
+            pltpu.VMEM((4 * CAP, SUB, LANES), BF16),
             pltpu.VMEM((2, 128, SUB, LANES), BF16),
             pltpu.VMEM((2, 8, 128), jnp.int32),
             pltpu.SMEM((2, 8, 128), jnp.int32),

time: 80.6 us -> 79.1 us (0.981); the launches traced: 79.2 us -> 78.8 us
  no operation moved by 1% of the time
where the time goes in v6:
time: 79.1 us; the launch traced here: 78.8 us
  Pallas kernels  78 us (99%)
  local copies, waits for them, and re-layouts  0.8 us (1%)
    pallas_call x1, Pallas kernels, shards(): pl.pallas_call(kernel, out_shape=jax.ShapeDtypeStruct((128, 2048), BF16),...  78 us

profile of v6, /device:TPU:32, one launch (start us, length us, event | category | flops | bytes accessed | tf_op | source)
XLA Modules:
  0.0 78.8 jit_solution(1564150333146784192)
XLA Ops:
  0.0 78.0 %shard_map.100 = bf16[128,2048]{1,0:T(8,128)(2,1)S(1)} custom-call(s32[2,128]{1,0:T(2,128)} %bitcast.12, f32[2,128]{1,0:T(2,128)} %bitcast.13, bf16[128,2048]{1,0:T(8,128)(2,1)} %tok_hbm.1, f32[1,2048]{1,0:T(1,128)} %bitcast.10, f32[16,128]{1,0:T(8,128)} %bitcast.11, bf16[2048,512]{1,0:T(8,128)(2,1)} %bitcast.7, bf16[2048,512]{1,0:T(8,128)(2,1)} %bitcast.8, ...), custom_call_target="tpu_custom_call" | custom-call | tf_op jit(solution)/shard_map/pallas_call | solution.py:484
  78.0 0.8 %copy.12 = bf16[128,2048]{1,0:T(8,128)(2,1)} copy(bf16[128,2048]{1,0:T(8,128)(2,1)S(1)} %shard_map.100) | data formatting | bytes 1048576
